TPU v7x, 32 devices: a whole 2x2x4 slice. The times are simulated.
32 devices in a mesh: ep: 4 (over y, x), tp: 8 (over z, core).
Axes of the slice: x: 2, y: 2, z: 4, core: 2. Of those that a mesh axis runs over, the one named last changes fastest.
Arguments:
- tokens: bfloat16 [2048, 2048], P('ep', 'tp'), may hold values from -6 to 6
- norm_gain: float32 [2048], replicated, may hold values from 0.1 to 1.9
- norm_shift: float32 [2048], replicated, may hold values from -3 to 3
- expert_ids: int32 [2048, 6], P('ep'), may hold values from 0 to 31, all different within a row; in each aligned block of 64 rows (0 to 63, 64 to 127, ...) at most 24 rows name the same one
- affinity: float32 [2048, 6], P('ep'), may hold values from 0.05 to 1
- expert_gate: bfloat16 [32, 2048, 512], P(('ep', 'tp')), may hold values from -0.125 to 0.125
- expert_up: bfloat16 [32, 2048, 512], P(('ep', 'tp')), may hold values from -0.125 to 0.125
- expert_down: bfloat16 [32, 512, 2048], P(('ep', 'tp')), may hold values from -0.25 to 0.25
- shared_gate: bfloat16 [512, 2048], P('tp'), may hold values from -0.125 to 0.125
- shared_up: bfloat16 [512, 2048], P('tp'), may hold values from -0.125 to 0.125
- shared_down: bfloat16 [512, 2048], replicated, may hold values from -0.25 to 0.25
Outputs:
- mixed: bfloat16 [2048, 2048], P(('ep', 'tp'))
Inputs may be any that keep to these rules, and one draw needn't show every extreme that they name: `expert_ids`: each row names 6 different experts; in each aligned block of 64 rows (the rows of one device of tp) no expert is named more than 24 times, and in some blocks an expert is named exactly 24 times.
All inputs are finite; a program needn't handle non-finite values.
Results may differ from a plain program's by a relative error of at most 0.0069.
Values may be sent and summed in bfloat16 or wider, within the bound.
A program may use at most 64 MiB of HBM per device.

v0:
```python
import functools
import math

import jax
import jax.numpy as jnp
from jax import lax
from jax.experimental import pallas as pl
from jax.experimental.pallas import tpu as pltpu
from jax.sharding import PartitionSpec as P

ROUTED_SCALE = 2.5
EPSILON = 1e-05
MESH = pl.DeviceIdType.MESH
F32 = jnp.float32
BF16 = jnp.bfloat16


def partner(index, step, count):
    if count & (count - 1):
        return lax.rem(index + step, count)
    result, bit = 0, 1
    while bit < count:
        result = result + ((index // bit) % 2 + (step // bit) % 2) % 2 * bit
        bit *= 2
    return result


def layer_kernel(
    sizes,
    tokens_ref,
    ids_ref,
    affinity_ref,
    gain_ref,
    shift_ref,
    sgate_ref,
    sup_ref,
    gate_hbm,
    up_hbm,
    down_hbm,
    sdown_hbm,
    out_ref,
    gate_ref,
    up_ref,
    down_ref,
    sdown_ref,
    whole,
    pick,
    spread_t,
    spread,
    sent,
    inc,
    norm,
    hidden,
    shidden,
    res,
    ret,
    part,
    own,
    pair_out,
    pair_in,
    far_out,
    far_in,
    load_sem,
    a_send,
    f_send,
    a_recv,
    b_send,
    b_recv,
    r_send,
    r_recv,
    p_send,
    p_recv,
    q_send,
    q_recv,
):
    ep, tp, rows, slots, slot_cap, feat, chunks, cols = sizes
    chips = tp // 2
    g = lax.axis_index("ep")
    t = lax.axis_index("tp")
    z = t // 2
    c = t % 2
    mate = z * 2 + 1 - c
    width = tp * feat
    shared_rows = sdown_ref.shape[0]

    loads = [
        pltpu.make_async_copy(gate_hbm, gate_ref, load_sem.at[0]),
        pltpu.make_async_copy(up_hbm, up_ref, load_sem.at[1]),
        pltpu.make_async_copy(down_hbm, down_ref, load_sem.at[2]),
        pltpu.make_async_copy(
            sdown_hbm.at[pl.ds(pl.multiple_of(t * shared_rows, 8), shared_rows)],
            sdown_ref,
            load_sem.at[3],
        ),
    ]
    for load in loads:
        load.start()

    def remote(src, dst, send, recv, e, k):
        return pltpu.make_async_remote_copy(
            src_ref=src,
            dst_ref=dst,
            send_sem=send,
            recv_sem=recv,
            device_id=(e, k),
            device_id_type=MESH,
        )

    barrier = pltpu.get_barrier_semaphore()
    partners = [(partner(g, p, ep), t) for p in range(1, ep)]
    partners += [(g, partner(z, d, chips) * 2 + c) for d in range(1, chips)]
    partners += [(g, mate)]
    for e, k in partners:
        pl.semaphore_signal(barrier, inc=1, device_id=(e, k), device_id_type=MESH)
    ids = ids_ref[...]
    affinity = affinity_ref[...]
    weights = affinity / jnp.sum(affinity, axis=0, keepdims=True) * ROUTED_SCALE
    block = rows // tp
    early = lax.broadcasted_iota(jnp.int32, (rows, rows), 0)
    late = lax.broadcasted_iota(jnp.int32, (rows, rows), 1)
    before = jnp.where((early < late) & (early // block == late // block), 1.0, 0.0).astype(BF16)
    hits = [ids == e * tp + t for e in range(ep)]
    chosen = [jnp.sum(jnp.where(hit, 1.0, 0.0), axis=0, keepdims=True) for hit in hits]
    pad = [jnp.zeros((-ep % 16, rows), F32)] if ep % 16 else []
    ranks = jnp.dot(
        jnp.concatenate(chosen + pad, axis=0).astype(BF16), before, preferred_element_type=F32
    ).astype(jnp.int32)
    base = lax.broadcasted_iota(jnp.int32, (1, rows), 1) // block * slot_cap
    line = lax.broadcasted_iota(jnp.int32, (slots, rows), 0)
    for e in range(ep):
        place = jnp.where(chosen[e] > 0.5, base + ranks[e : e + 1, :], -1)
        weight = jnp.sum(jnp.where(hits[e], weights, 0.0), axis=0, keepdims=True)
        pick[e] = jnp.where(line == place, 1.0, 0.0).astype(BF16)
        spread_t[pl.ds(e * slots, slots), :] = jnp.where(line == place, weight, 0.0)
    pl.semaphore_wait(barrier, len(partners))

    first = []
    first.append(remote(tokens_ref, whole.at[t], f_send.at[0], a_recv.at[t], g, mate))
    for d in range(1, chips):
        there = partner(z, d, chips) * 2 + c
        first.append(remote(tokens_ref, whole.at[t], a_send.at[d], a_recv.at[t], g, there))
    for copy in first:
        copy.start()
    whole[t] = tokens_ref[...]

    def forward(k, d):
        return remote(whole.at[k], whole.at[k], f_send.at[d], a_recv.at[k], g, mate)

    def chunk_at(i):
        d = i // 2
        side = i % 2
        return d, side, partner(z, d, chips) * 2 + lax.rem(c + side, 2)

    near = [p for p in range(1, ep) if not p & (p - 1)]
    far = [p for p in range(1, ep) if p & (p - 1)]
    lag = 3 * tp // 8
    half = chunks // 8

    def send_rows(k, p):
        e = partner(g, p, ep)
        remote(sent.at[k, e], inc.at[k, g], b_send, b_recv.at[g], e, t).start()

    def chunk_step(i, carry):
        d, side, k = chunk_at(i)

        @pl.when(i > 0)
        def _():
            forward(k, d).wait_recv()

        @pl.when((i > 0) & (side == 0))
        def _():
            forward(k, d).start()

        picked = jnp.dot(
            pick[...].reshape(ep * slots, rows), whole[k], preferred_element_type=F32
        ).astype(BF16)
        sent[k] = picked.reshape(ep, slots, feat)
        inc[k, g] = sent[k, g]
        for p in near:
            send_rows(k, p)
        if far:

            @pl.when(i >= lag)
            def _():
                for p in far:
                    send_rows(chunk_at(i - lag)[2], p)

        return carry

    lax.fori_loop(0, tp, chunk_step, 0)

    def late_step(i, carry):
        for p in far:
            send_rows(chunk_at(i)[2], p)
        return carry

    if far:
        lax.fori_loop(tp - lag, tp, late_step, 0)
    spread[...] = spread_t[...].T.astype(BF16)

    def normalise(read, count):
        tile = math.gcd(64, count)

        def body(i, carry):
            at = pl.ds(pl.multiple_of(i * tile, tile), tile)
            total = jnp.zeros((tile, feat), F32)
            for k in range(tp):
                total = total + read(k, at).astype(F32)
            mean = jnp.sum(total, axis=1, keepdims=True) / width
            total = jnp.zeros((tile, feat), F32)
            for k in range(tp):
                center = read(k, at).astype(F32) - mean
                total = total + center * center
            scale = lax.rsqrt(jnp.sum(total, axis=1, keepdims=True) / width + EPSILON)
            for k in range(tp):
                lanes = slice(k * feat, (k + 1) * feat)
                value = (read(k, at).astype(F32) - mean) * scale
                value = value * gain_ref[:, lanes] + shift_ref[:, lanes]
                norm[at, lanes] = value.astype(BF16)
            return carry

        lax.fori_loop(0, count // tile, body, 0)

    normalise(lambda k, at: whole[k, at, :], rows)
    contract = (((1,), (1,)), ((), ()))
    sg = lax.dot_general(norm[...], sgate_ref[...], contract, preferred_element_type=F32)
    su = lax.dot_general(norm[...], sup_ref[...], contract, preferred_element_type=F32)
    shidden[...] = (jax.nn.silu(sg) * su).astype(BF16)

    for load in loads:
        load.wait()

    def expert_step(p, carry):
        s = partner(g, p, ep)

        @pl.when(p > 0)
        def _():
            remote(sent.at[:, s], inc.at[:, s], b_send, b_recv.at[s], s, t).wait_recv()

        normalise(lambda k, at: inc[k, s, at, :], slots)
        got = norm[0:slots, :]
        gate_act = jnp.dot(got, gate_ref[...], preferred_element_type=F32)
        up_act = jnp.dot(got, up_ref[...], preferred_element_type=F32)
        hidden[s] = (jax.nn.silu(gate_act) * up_act).astype(BF16)

        @pl.when(p == 0)
        def _():
            def own_step(i, carry):
                ret[i, g] = down_rows(i, g)
                return carry

            lax.fori_loop(0, chunks, own_step, 0)

        is_near = functools.reduce(jnp.logical_or, [p == n for n in near])

        @pl.when(is_near)
        def _():
            def near_step(i, carry):
                send_result(i, s)
                return carry

            lax.fori_loop(0, half, near_step, 0)

        return carry

    def lanes_of(i):
        return pl.ds(pl.multiple_of(i * cols, cols), cols)

    def down_rows(i, s):
        return jnp.dot(
            hidden[s], down_ref[:, lanes_of(i)], preferred_element_type=F32
        ).astype(BF16)

    def send_result(i, s):
        res[i, s] = down_rows(i, s)
        remote(res.at[i, s], ret.at[i, g], r_send, r_recv.at[i], s, t).start()

    lax.fori_loop(0, ep, expert_step, 0)

    def down_step(i, carry):
        for p in far:
            send_result(i, partner(g, p, ep))

        @pl.when(i < chunks - half)
        def _():
            for p in near:
                send_result(i + half, partner(g, p, ep))

        return carry

    lax.fori_loop(0, chunks, down_step, 0)

    def pair_copy(i):
        return remote(pair_out.at[i], pair_in.at[i], p_send, p_recv.at[i], g, mate)

    def produce(i):
        others = pl.ds(0, ep - 1)
        remote(res.at[i, others], ret.at[i, others], r_send, r_recv.at[i], g, mate).wait_recv()
        total = jnp.dot(
            spread[...], ret[i].reshape(ep * slots, cols), preferred_element_type=F32
        ) + jnp.dot(shidden[...], sdown_ref[:, lanes_of(i)], preferred_element_type=F32)
        part[i % 2] = total.reshape(part.shape[1:])
        for zz in range(chips):
            pair_out[i, zz] = part[i % 2, zz * 2 + 1 - c].astype(BF16)
        pair_copy(i).start()

    def finish(i):
        pair_copy(i).wait_recv()
        for d in range(1, chips):
            zz = partner(z, d, chips)
            far_out[i, zz] = (part[i % 2, zz * 2 + c] + pair_in[i, zz].astype(F32)).astype(BF16)
            remote(
                far_out.at[i, zz],
                far_in.at[i, z],
                q_send,
                q_recv,
                g,
                zz * 2 + c,
            ).start()
        own[i] = part[i % 2, t] + pair_in[i, z].astype(F32)

    def sum_step(i, carry):
        @pl.when(i < chunks)
        def _():
            produce(i)

        @pl.when(i > 0)
        def _():
            finish(i - 1)

        return carry

    lax.fori_loop(0, chunks + 1, sum_step, 0)

    rest = pl.ds(0, chips - 1)
    remote(far_out.at[:, rest], far_in.at[:, rest], q_send, q_recv, g, mate).wait()

    def out_step(i, carry):
        total = own[i]
        for d in range(1, chips):
            total = total + far_in[i, partner(z, d, chips)].astype(F32)
        out_ref[:, lanes_of(i)] = total.astype(BF16)
        return carry

    lax.fori_loop(0, chunks, out_step, 0)

    others = pl.ds(0, ep - 1)
    remote(sent.at[:, others], inc.at[:, others], b_send, b_recv.at[g], g, mate).wait_send()
    remote(res.at[:, others], ret.at[:, others], r_send, r_recv.at[0], g, mate).wait_send()
    remote(pair_out, pair_in, p_send, p_recv.at[0], g, mate).wait_send()
    for copy in first:
        copy.wait_send()
    for d in range(1, chips):
        k = partner(z, d, chips) * 2 + c
        forward(k, d).wait_send()


def on_device(
    tokens,
    norm_gain,
    norm_shift,
    expert_ids,
    affinity,
    expert_gate,
    expert_up,
    expert_down,
    shared_gate,
    shared_up,
    shared_down,
):
    ep = lax.axis_size("ep")
    tp = lax.axis_size("tp")
    rows, feat = tokens.shape
    width = feat * tp
    top_count = expert_ids.shape[1]
    block = rows // tp
    expert_count = ep * tp
    slot_cap = max(1, 2 * block * top_count // expert_count)
    slots = tp * slot_cap
    hid = expert_gate.shape[2]
    shared_rows = shared_gate.shape[0]
    cols = 256
    chunks = width // cols
    chips = tp // 2

    vmem = pl.BlockSpec(memory_space=pltpu.VMEM)
    anywhere = pl.BlockSpec(memory_space=pl.ANY)
    dma = pltpu.SemaphoreType.DMA
    return pl.pallas_call(
        functools.partial(layer_kernel, (ep, tp, rows, slots, slot_cap, feat, chunks, cols)),
        out_shape=jax.ShapeDtypeStruct((block, width), BF16),
        in_specs=[vmem] * 7 + [anywhere] * 4,
        out_specs=vmem,
        scratch_shapes=[
            pltpu.VMEM((width, hid), BF16),
            pltpu.VMEM((width, hid), BF16),
            pltpu.VMEM((hid, width), BF16),
            pltpu.VMEM((shared_rows, width), BF16),
            pltpu.VMEM((tp, rows, feat), BF16),
            pltpu.VMEM((ep, slots, rows), BF16),
            pltpu.VMEM((ep * slots, rows), F32),
            pltpu.VMEM((rows, ep * slots), BF16),
            pltpu.VMEM((tp, ep, slots, feat), BF16),
            pltpu.VMEM((tp, ep, slots, feat), BF16),
            pltpu.VMEM((max(rows, slots), width), BF16),
            pltpu.VMEM((ep, slots, hid), BF16),
            pltpu.VMEM((rows, shared_rows), BF16),
            pltpu.VMEM((chunks, ep, slots, cols), BF16),
            pltpu.VMEM((chunks, ep, slots, cols), BF16),
            pltpu.VMEM((2, tp, block, cols), F32),
            pltpu.VMEM((chunks, block, cols), F32),
            pltpu.VMEM((chunks, chips, block, cols), BF16),
            pltpu.VMEM((chunks, chips, block, cols), BF16),
            pltpu.VMEM((chunks, chips, block, cols), BF16),
            pltpu.VMEM((chunks, chips, block, cols), BF16),
            dma((4,)),
            dma((chips,)),
            dma((chips,)),
            dma((tp,)),
            dma,
            dma((ep,)),
            dma,
            dma((chunks,)),
            dma,
            dma((chunks,)),
            dma,
            dma,
        ],
        compiler_params=pltpu.CompilerParams(
            collective_id=0, has_side_effects=True, vmem_limit_bytes=56 * 1024 * 1024
        ),
        name="moe_layer",
    )(
        tokens,
        expert_ids.T,
        affinity.T,
        norm_gain.reshape(1, width),
        norm_shift.reshape(1, width),
        shared_gate,
        shared_up,
        expert_gate[0],
        expert_up[0],
        expert_down[0],
        shared_down,
    )


def solution(mesh):
    placed = (
        P("ep", "tp"),
        P(),
        P(),
        P("ep", None),
        P("ep", None),
        P(("ep", "tp"), None, None),
        P(("ep", "tp"), None, None),
        P(("ep", "tp"), None, None),
        P("tp", None),
        P("tp", None),
        P(),
    )
    return jax.shard_map(
        on_device, mesh=mesh, in_specs=placed, out_specs=P(("ep", "tp"), None), check_vma=False
    )
```

profile of v0, /device:TPU:0, one launch (start us, length us, event | category | flops | bytes accessed | tf_op | source)
XLA Modules:
  0.0 96.0 jit_solution(14248648144517472797)
XLA Ops:
  0.0 94.3 %moe_layer.1 = bf16[64,2048]{1,0:T(8,128)(2,1)} custom-call(bf16[512,256]{1,0:T(8,128)(2,1)} %tokens_ref.1, s32[6,512]{1,0:T(8,128)} %bitcast.10, f32[6,512]{1,0:T(8,128)} %bitcast.11, f32[1,2048]{1,0:T(1,128)} %bitcast.12, f32[1,2048]{1,0:T(1,128)} %bitcast.13, bf16[64,2048]{1,0:T(8,128)(2,1)} %sgate_ref.1, bf16[64,2048]{1,0:T(8,128)(2,1)} %sup_ref.1, ...), custom_call_target="tpu_custom_call" | custom-call | tf_op jit(solution)/shard_map/moe_layer/pallas_call | solution.py:389
  94.3 1.7 %copy.13 = bf16[64,2048]{1,0:T(8,128)(2,1)} copy(bf16[64,2048]{1,0:T(8,128)(2,1)} %moe_layer.1) | data formatting | bytes 524288
where the time goes:
time: 96.1 us; the launch traced here: 96 us
  Pallas kernels  94.3 us (98%)
  local copies, waits for them, and re-layouts  1.67 us (2%)
    pallas_call x1, Pallas kernels, on_device(): pl.pallas_call(functools.partial(layer_kernel, (ep, tp, rows, slots, slot...  94.3 us

commit v1 on v0

--- a/solution.py
+++ b/solution.py
@@ -27,18 +27,24 @@
 
 def layer_kernel(
     sizes,
-    tokens_ref,
+    tokens_hbm,
+    ids_hbm,
+    affinity_hbm,
+    gain_hbm,
+    shift_hbm,
+    sgate_hbm,
+    sup_hbm,
+    gate_hbm,
+    up_hbm,
+    down_hbm,
+    sdown_hbm,
+    out_ref,
     ids_ref,
     affinity_ref,
     gain_ref,
     shift_ref,
     sgate_ref,
     sup_ref,
-    gate_hbm,
-    up_hbm,
-    down_hbm,
-    sdown_hbm,
-    out_ref,
     gate_ref,
     up_ref,
     down_ref,
@@ -61,7 +67,9 @@
     far_out,
     far_in,
     load_sem,
-    a_send,
+    first_sem,
+    u_send,
+    d_send,
     f_send,
     a_recv,
     b_send,
@@ -83,17 +91,26 @@
     width = tp * feat
     shared_rows = sdown_ref.shape[0]
 
+    firsts = [
+        pltpu.make_async_copy(ids_hbm, ids_ref, first_sem.at[0]),
+        pltpu.make_async_copy(affinity_hbm, affinity_ref, first_sem.at[1]),
+        pltpu.make_async_copy(tokens_hbm, whole.at[t], first_sem.at[2]),
+    ]
     loads = [
-        pltpu.make_async_copy(gate_hbm, gate_ref, load_sem.at[0]),
-        pltpu.make_async_copy(up_hbm, up_ref, load_sem.at[1]),
-        pltpu.make_async_copy(down_hbm, down_ref, load_sem.at[2]),
+        pltpu.make_async_copy(gain_hbm, gain_ref, load_sem.at[0]),
+        pltpu.make_async_copy(shift_hbm, shift_ref, load_sem.at[1]),
+        pltpu.make_async_copy(sgate_hbm, sgate_ref, load_sem.at[2]),
+        pltpu.make_async_copy(sup_hbm, sup_ref, load_sem.at[3]),
         pltpu.make_async_copy(
             sdown_hbm.at[pl.ds(pl.multiple_of(t * shared_rows, 8), shared_rows)],
             sdown_ref,
-            load_sem.at[3],
+            load_sem.at[4],
         ),
+        pltpu.make_async_copy(gate_hbm, gate_ref, load_sem.at[5]),
+        pltpu.make_async_copy(up_hbm, up_ref, load_sem.at[6]),
+        pltpu.make_async_copy(down_hbm, down_ref, load_sem.at[7]),
     ]
-    for load in loads:
+    for load in firsts:
         load.start()
 
     def remote(src, dst, send, recv, e, k):
@@ -112,6 +129,10 @@
     partners += [(g, mate)]
     for e, k in partners:
         pl.semaphore_signal(barrier, inc=1, device_id=(e, k), device_id_type=MESH)
+    for load in loads:
+        load.start()
+    for load in firsts[:2]:
+        load.wait()
     ids = ids_ref[...]
     affinity = affinity_ref[...]
     weights = affinity / jnp.sum(affinity, axis=0, keepdims=True) * ROUTED_SCALE
@@ -134,22 +155,38 @@
         spread_t[pl.ds(e * slots, slots), :] = jnp.where(line == place, weight, 0.0)
     pl.semaphore_wait(barrier, len(partners))
 
-    first = []
-    first.append(remote(tokens_ref, whole.at[t], f_send.at[0], a_recv.at[t], g, mate))
-    for d in range(1, chips):
-        there = partner(z, d, chips) * 2 + c
-        first.append(remote(tokens_ref, whole.at[t], a_send.at[d], a_recv.at[t], g, there))
-    for copy in first:
-        copy.start()
-    whole[t] = tokens_ref[...]
-
-    def forward(k, d):
-        return remote(whole.at[k], whole.at[k], f_send.at[d], a_recv.at[k], g, mate)
+    def forward(k):
+        return remote(whole.at[k], whole.at[k], f_send.at[k // 2], a_recv.at[k], g, mate)
+
+    def upward(k):
+        there = lax.rem(z + 1, chips) * 2 + c
+        return remote(whole.at[k], whole.at[k], u_send.at[k // 2], a_recv.at[k], g, there)
+
+    def downward(k):
+        there = lax.rem(z + chips - 1, chips) * 2 + c
+        return remote(whole.at[k], whole.at[k], d_send.at[k // 2], a_recv.at[k], g, there)
+
+    firsts[2].wait()
+
+    @pl.when(z < chips - 1)
+    def _():
+        upward(t).start()
+
+    @pl.when(z > 0)
+    def _():
+        downward(t).start()
+
+    forward(t).start()
+
+    both = jnp.minimum(z, chips - 1 - z)
+    longer = jnp.where(z > chips - 1 - z, -1, 1)
 
     def chunk_at(i):
-        d = i // 2
+        j = i // 2
         side = i % 2
-        return d, side, partner(z, d, chips) * 2 + lax.rem(c + side, 2)
+        alternate = (j + 1) // 2 * (j % 2 * 2 - 1)
+        step = jnp.where(j <= 2 * both, alternate, longer * (j - both))
+        return side, z + step, (z + step) * 2 + lax.rem(c + side, 2)
 
     near = [p for p in range(1, ep) if not p & (p - 1)]
     far = [p for p in range(1, ep) if p & (p - 1)]
@@ -161,15 +198,25 @@
         remote(sent.at[k, e], inc.at[k, g], b_send, b_recv.at[g], e, t).start()
 
     def chunk_step(i, carry):
-        d, side, k = chunk_at(i)
+        side, chip, k = chunk_at(i)
 
         @pl.when(i > 0)
         def _():
-            forward(k, d).wait_recv()
-
-        @pl.when((i > 0) & (side == 0))
-        def _():
-            forward(k, d).start()
+            forward(k).wait_recv()
+
+        fresh = (i > 0) & (side == 0)
+
+        @pl.when(fresh & (chip < z) & (z < chips - 1))
+        def _():
+            upward(k).start()
+
+        @pl.when(fresh & (chip > z) & (z > 0))
+        def _():
+            downward(k).start()
+
+        @pl.when(fresh)
+        def _():
+            forward(k).start()
 
         picked = jnp.dot(
             pick[...].reshape(ep * slots, rows), whole[k], preferred_element_type=F32
@@ -221,13 +268,15 @@
 
         lax.fori_loop(0, count // tile, body, 0)
 
+    for load in loads[:5]:
+        load.wait()
     normalise(lambda k, at: whole[k, at, :], rows)
     contract = (((1,), (1,)), ((), ()))
     sg = lax.dot_general(norm[...], sgate_ref[...], contract, preferred_element_type=F32)
     su = lax.dot_general(norm[...], sup_ref[...], contract, preferred_element_type=F32)
     shidden[...] = (jax.nn.silu(sg) * su).astype(BF16)
 
-    for load in loads:
+    for load in loads[5:]:
         load.wait()
 
     def expert_step(p, carry):
@@ -348,11 +397,22 @@
     remote(sent.at[:, others], inc.at[:, others], b_send, b_recv.at[g], g, mate).wait_send()
     remote(res.at[:, others], ret.at[:, others], r_send, r_recv.at[0], g, mate).wait_send()
     remote(pair_out, pair_in, p_send, p_recv.at[0], g, mate).wait_send()
-    for copy in first:
-        copy.wait_send()
-    for d in range(1, chips):
-        k = partner(z, d, chips) * 2 + c
-        forward(k, d).wait_send()
+
+    def sent_step(chip, carry):
+        k = chip * 2 + c
+        forward(k).wait_send()
+
+        @pl.when((chip <= z) & (z < chips - 1))
+        def _():
+            upward(k).wait_send()
+
+        @pl.when((chip >= z) & (z > 0))
+        def _():
+            downward(k).wait_send()
+
+        return carry
+
+    lax.fori_loop(0, chips, sent_step, 0)
 
 
 def on_device(
@@ -389,9 +449,15 @@
     return pl.pallas_call(
         functools.partial(layer_kernel, (ep, tp, rows, slots, slot_cap, feat, chunks, cols)),
         out_shape=jax.ShapeDtypeStruct((block, width), BF16),
-        in_specs=[vmem] * 7 + [anywhere] * 4,
+        in_specs=[anywhere] * 11,
         out_specs=vmem,
         scratch_shapes=[
+            pltpu.VMEM((top_count, rows), jnp.int32),
+            pltpu.VMEM((top_count, rows), F32),
+            pltpu.VMEM((1, width), F32),
+            pltpu.VMEM((1, width), F32),
+            pltpu.VMEM((shared_rows, width), BF16),
+            pltpu.VMEM((shared_rows, width), BF16),
             pltpu.VMEM((width, hid), BF16),
             pltpu.VMEM((width, hid), BF16),
             pltpu.VMEM((hid, width), BF16),
@@ -413,7 +479,9 @@
             pltpu.VMEM((chunks, chips, block, cols), BF16),
             pltpu.VMEM((chunks, chips, block, cols), BF16),
             pltpu.VMEM((chunks, chips, block, cols), BF16),
-            dma((4,)),
+            dma((8,)),
+            dma((3,)),
+            dma((chips,)),
             dma((chips,)),
             dma((chips,)),
             dma((tp,)),

time: 96.1 us -> 93.6 us (0.974)
  Pallas kernels: 94.3 us -> 91.7 us
    pallas_call x1, Pallas kernels: 94.3 us -> 91.7 us  [on_device(): pl.pallas_call(functools.partial(layer_kernel, (ep, tp, rows, slots, slot...]
where the time goes in v1:
time: 93.6 us; the launch traced here: 93.4 us
  Pallas kernels  91.7 us (98%)
  local copies, waits for them, and re-layouts  1.67 us (2%)
    pallas_call x1, Pallas kernels, on_device(): pl.pallas_call(functools.partial(layer_kernel, (ep, tp, rows, slots, slot...  91.7 us

profile of v1, /device:TPU:0, one launch (start us, length us, event | category | flops | bytes accessed | tf_op | source)
XLA Modules:
  0.0 93.4 jit_solution(10965052128429928863)
XLA Ops:
  0.0 91.7 %moe_layer.1 = bf16[64,2048]{1,0:T(8,128)(2,1)} custom-call(bf16[512,256]{1,0:T(8,128)(2,1)} %tokens_hbm.1, s32[6,512]{1,0:T(8,128)} %bitcast.10, f32[6,512]{1,0:T(8,128)} %bitcast.11, f32[1,2048]{1,0:T(1,128)} %bitcast.12, f32[1,2048]{1,0:T(1,128)} %bitcast.13, bf16[64,2048]{1,0:T(8,128)(2,1)} %sgate_hbm.1, bf16[64,2048]{1,0:T(8,128)(2,1)} %sup_hbm.1, ...), custom_call_target="tpu_custom_call" | custom-call | tf_op jit(solution)/shard_map/moe_layer/pallas_call | solution.py:449
  91.7 1.7 %copy.13 = bf16[64,2048]{1,0:T(8,128)(2,1)} copy(bf16[64,2048]{1,0:T(8,128)(2,1)} %moe_layer.1) | data formatting | bytes 524288

commit v2 on v1

--- a/solution.py
+++ b/solution.py
@@ -178,71 +178,77 @@
 
     forward(t).start()
 
-    both = jnp.minimum(z, chips - 1 - z)
-    longer = jnp.where(z > chips - 1 - z, -1, 1)
-
-    def chunk_at(i):
-        j = i // 2
-        side = i % 2
-        alternate = (j + 1) // 2 * (j % 2 * 2 - 1)
-        step = jnp.where(j <= 2 * both, alternate, longer * (j - both))
-        return side, z + step, (z + step) * 2 + lax.rem(c + side, 2)
-
     near = [p for p in range(1, ep) if not p & (p - 1)]
     far = [p for p in range(1, ep) if p & (p - 1)]
-    lag = 3 * tp // 8
     half = chunks // 8
 
     def send_rows(k, p):
         e = partner(g, p, ep)
         remote(sent.at[k, e], inc.at[k, g], b_send, b_recv.at[g], e, t).start()
 
-    def chunk_step(i, carry):
-        side, chip, k = chunk_at(i)
-
-        @pl.when(i > 0)
-        def _():
-            forward(k).wait_recv()
-
-        fresh = (i > 0) & (side == 0)
-
-        @pl.when(fresh & (chip < z) & (z < chips - 1))
+    def arrive(chip):
+        k = chip * 2 + c
+        forward(k).wait_recv()
+
+        @pl.when((chip < z) & (z < chips - 1))
         def _():
             upward(k).start()
 
-        @pl.when(fresh & (chip > z) & (z > 0))
+        @pl.when((chip > z) & (z > 0))
         def _():
             downward(k).start()
 
-        @pl.when(fresh)
-        def _():
-            forward(k).start()
-
-        picked = jnp.dot(
-            pick[...].reshape(ep * slots, rows), whole[k], preferred_element_type=F32
-        ).astype(BF16)
-        sent[k] = picked.reshape(ep, slots, feat)
-        inc[k, g] = sent[k, g]
-        for p in near:
-            send_rows(k, p)
-        if far:
-
-            @pl.when(i >= lag)
+        forward(k).start()
+
+    def distance_step(d, carry):
+        def at_side(side):
+            chip = z + d * (side * 2 - 1)
+            return chip, (chip >= 0) & (chip < chips) & ((d > 0) | (side == 0))
+
+        for side in range(2):
+            chip, there = at_side(side)
+
+            @pl.when(there & (d > 0))
+            def _():
+                arrive(chip)
+
+        def chunk_step(q, carry):
+            chip, there = at_side(q % 2)
+            lane = q // 2
+            k = chip * 2 + lax.rem(c + lane, 2)
+
+            @pl.when(there)
+            def _():
+                @pl.when(lane > 0)
+                def _():
+                    forward(k).wait_recv()
+
+                picked = jnp.dot(
+                    pick[...].reshape(ep * slots, rows), whole[k], preferred_element_type=F32
+                ).astype(BF16)
+                sent[k] = picked.reshape(ep, slots, feat)
+                inc[k, g] = sent[k, g]
+                for p in near:
+                    send_rows(k, p)
+
+            return carry
+
+        lax.fori_loop(0, 4, chunk_step, 0)
+
+        def far_step(q, carry):
+            chip, there = at_side(q % 2)
+
+            @pl.when(there)
             def _():
                 for p in far:
-                    send_rows(chunk_at(i - lag)[2], p)
-
+                    send_rows(chip * 2 + lax.rem(c + q // 2, 2), p)
+
+            return carry
+
+        lax.fori_loop(0, 4, far_step, 0)
         return carry
 
-    lax.fori_loop(0, tp, chunk_step, 0)
-
-    def late_step(i, carry):
-        for p in far:
-            send_rows(chunk_at(i)[2], p)
-        return carry
-
-    if far:
-        lax.fori_loop(tp - lag, tp, late_step, 0)
+    lax.fori_loop(0, chips, distance_step, 0)
     spread[...] = spread_t[...].T.astype(BF16)
 
     def normalise(read, count):

time: 93.6 us -> 88.3 us (0.943)
  Pallas kernels: 91.7 us -> 86.4 us
    pallas_call x1, Pallas kernels: 91.7 us -> 86.4 us  [on_device(): pl.pallas_call(functools.partial(layer_kernel, (ep, tp, rows, slots, slot...]
where the time goes in v2:
time: 88.3 us; the launch traced here: 88.1 us
  Pallas kernels  86.4 us (98%)
  local copies, waits for them, and re-layouts  1.67 us (2%)
    pallas_call x1, Pallas kernels, on_device(): pl.pallas_call(functools.partial(layer_kernel, (ep, tp, rows, slots, slot...  86.4 us

profile of v2, /device:TPU:0, one launch (start us, length us, event | category | flops | bytes accessed | tf_op | source)
XLA Modules:
  0.0 88.1 jit_solution(15631553501747692440)
XLA Ops:
  0.0 86.4 %moe_layer.1 = bf16[64,2048]{1,0:T(8,128)(2,1)} custom-call(bf16[512,256]{1,0:T(8,128)(2,1)} %tokens_hbm.1, s32[6,512]{1,0:T(8,128)} %bitcast.10, f32[6,512]{1,0:T(8,128)} %bitcast.11, f32[1,2048]{1,0:T(1,128)} %bitcast.12, f32[1,2048]{1,0:T(1,128)} %bitcast.13, bf16[64,2048]{1,0:T(8,128)(2,1)} %sgate_hbm.1, bf16[64,2048]{1,0:T(8,128)(2,1)} %sup_hbm.1, ...), custom_call_target="tpu_custom_call" | custom-call | tf_op jit(solution)/shard_map/moe_layer/pallas_call | solution.py:455
  86.4 1.7 %copy.13 = bf16[64,2048]{1,0:T(8,128)(2,1)} copy(bf16[64,2048]{1,0:T(8,128)(2,1)} %moe_layer.1) | data formatting | bytes 524288

commit v3 on v2

--- a/solution.py
+++ b/solution.py
@@ -60,6 +60,9 @@
     shidden,
     res,
     ret,
+    ids_other,
+    extra,
+    pick_other,
     part,
     own,
     pair_out,
@@ -80,8 +83,16 @@
     p_recv,
     q_send,
     q_recv,
+    i_send,
+    i_recv,
+    x_send,
+    x_recv,
+    eu_send,
+    ed_send,
+    ef_send,
+    e_recv,
 ):
-    ep, tp, rows, slots, slot_cap, feat, chunks, cols = sizes
+    ep, tp, rows, slots, slot_cap, feat, chunks, cols, shift = sizes
     chips = tp // 2
     g = lax.axis_index("ep")
     t = lax.axis_index("tp")
@@ -146,7 +157,7 @@
     ranks = jnp.dot(
         jnp.concatenate(chosen + pad, axis=0).astype(BF16), before, preferred_element_type=F32
     ).astype(jnp.int32)
-    base = lax.broadcasted_iota(jnp.int32, (1, rows), 1) // block * slot_cap
+    base = (tp - 1 - lax.broadcasted_iota(jnp.int32, (1, rows), 1) // block) * slot_cap
     line = lax.broadcasted_iota(jnp.int32, (slots, rows), 0)
     for e in range(ep):
         place = jnp.where(chosen[e] > 0.5, base + ranks[e : e + 1, :], -1)
@@ -178,13 +189,80 @@
 
     forward(t).start()
 
+    crossed = slots - shift * slot_cap
+    extra_rows = shift * block
+
+    def ids_copy(p):
+        lanes = pl.ds(0, ids_other.shape[2])
+        e = partner(g, p, ep)
+        return remote(ids_ref.at[:, lanes], ids_other.at[p - 1], i_send, i_recv, e, t)
+
+    def extra_copy(p):
+        e = partner(g, p, ep)
+        rows_out = whole.at[t, pl.ds(0, extra_rows)]
+        return remote(rows_out, extra.at[t, p - 1], x_send, x_recv, e, t)
+
+    def extra_forward(k):
+        return remote(extra.at[k], extra.at[k], ef_send.at[k // 2], e_recv.at[k], g, mate)
+
+    def extra_upward(k):
+        there = lax.rem(z + 1, chips) * 2 + c
+        return remote(extra.at[k], extra.at[k], eu_send.at[k // 2], e_recv.at[k], g, there)
+
+    def extra_downward(k):
+        there = lax.rem(z + chips - 1, chips) * 2 + c
+        return remote(extra.at[k], extra.at[k], ed_send.at[k // 2], e_recv.at[k], g, there)
+
+    if shift:
+        for p in range(1, ep):
+            ids_copy(p).start()
+            extra_copy(p).start()
+
+    def extra_onward(chip):
+        k = chip * 2 + c
+
+        @pl.when((chip <= z) & (z < chips - 1))
+        def _():
+            extra_upward(k).start()
+
+        @pl.when((chip >= z) & (z > 0))
+        def _():
+            extra_downward(k).start()
+
+        extra_forward(k).start()
+
+    def pick_others():
+        remote(ids_other, ids_other, i_send, i_recv, g, mate).wait_recv()
+        lanes = ids_other.shape[2]
+        early = lax.broadcasted_iota(jnp.int32, (lanes, lanes), 0)
+        late = lax.broadcasted_iota(jnp.int32, (lanes, lanes), 1)
+        before = jnp.where((early < late) & (early // block == late // block), 1.0, 0.0)
+        chosen = [
+            jnp.sum(jnp.where(ids_other[p] == g * tp + t, 1.0, 0.0), axis=0, keepdims=True)
+            for p in range(ep - 1)
+        ]
+        pad = [jnp.zeros((-(ep - 1) % 16, lanes), F32)]
+        ranks = jnp.dot(
+            jnp.concatenate(chosen + pad, axis=0).astype(BF16),
+            before.astype(BF16),
+            preferred_element_type=F32,
+        ).astype(jnp.int32)
+        blocks = lax.broadcasted_iota(jnp.int32, (1, lanes), 1) // block
+        base = (shift - 1 - blocks) * slot_cap
+        line = lax.broadcasted_iota(jnp.int32, (shift * slot_cap, lanes), 0)
+        for p in range(ep - 1):
+            named = (chosen[p] > 0.5) & (blocks < shift)
+            place = jnp.where(named, base + ranks[p : p + 1, :], -1)
+            pick_other[p] = jnp.where(line == place, 1.0, 0.0).astype(BF16)
+
     near = [p for p in range(1, ep) if not p & (p - 1)]
     far = [p for p in range(1, ep) if p & (p - 1)]
     half = chunks // 8
 
     def send_rows(k, p):
         e = partner(g, p, ep)
-        remote(sent.at[k, e], inc.at[k, g], b_send, b_recv.at[g], e, t).start()
+        over = pl.ds(0, crossed)
+        remote(sent.at[k, e, over], inc.at[k, g, over], b_send, b_recv.at[g], e, t).start()
 
     def arrive(chip):
         k = chip * 2 + c
@@ -246,11 +324,45 @@
             return carry
 
         lax.fori_loop(0, 4, far_step, 0)
+        if not shift:
+            return carry
+
+        @pl.when(d == 0)
+        def _():
+            remote(extra.at[t], extra.at[t], x_send, x_recv, g, mate).wait_recv()
+            extra_onward(z)
+            pick_others()
+
+        for side in range(2):
+            chip, there = at_side(side)
+
+            @pl.when(there & (d > 0))
+            def _():
+                extra_forward(chip * 2 + c).wait_recv()
+                extra_onward(chip)
+
+        def extra_step(q, carry):
+            chip, there = at_side(q % 2)
+            lane = q // 2
+            k = chip * 2 + lax.rem(c + lane, 2)
+
+            @pl.when(there)
+            def _():
+                @pl.when(lane > 0)
+                def _():
+                    extra_forward(k).wait_recv()
+
+                for p in range(1, ep):
+                    inc[k, partner(g, p, ep), crossed:slots, :] = jnp.dot(
+                        pick_other[p - 1][:, :extra_rows], extra[k, p - 1], preferred_element_type=F32
+                    ).astype(BF16)
+
+            return carry
+
+        lax.fori_loop(0, 4, extra_step, 0)
         return carry
 
     lax.fori_loop(0, chips, distance_step, 0)
-    spread[...] = spread_t[...].T.astype(BF16)
-
     def normalise(read, count):
         tile = math.gcd(64, count)
 
@@ -274,76 +386,80 @@
 
         lax.fori_loop(0, count // tile, body, 0)
 
-    for load in loads[:5]:
+    for load in loads:
         load.wait()
+
+    def activate(s):
+        normalise(lambda k, at: inc[k, s, at, :], slots)
+        got = norm[0:slots, :]
+        gate_act = jnp.dot(got, gate_ref[...], preferred_element_type=F32)
+        up_act = jnp.dot(got, up_ref[...], preferred_element_type=F32)
+        hidden[s] = (jax.nn.silu(gate_act) * up_act).astype(BF16)
+
+    def expert_step(j, carry):
+        p = expert_order(j)
+        s = partner(g, p, ep)
+        over = pl.ds(0, crossed)
+        remote(sent.at[:, s, over], inc.at[:, s, over], b_send, b_recv.at[s], s, t).wait_recv()
+
+        activate(s)
+        is_near = functools.reduce(jnp.logical_or, [p == n for n in near])
+
+        @pl.when(is_near)
+        def _():
+            def near_step(i, carry):
+                send_result(i, s)
+                return carry
+
+            lax.fori_loop(0, half, near_step, 0)
+
+        return carry
+
+    def lanes_of(i):
+        return pl.ds(pl.multiple_of(i * cols, cols), cols)
+
+    def down_rows(i, s):
+        return jnp.dot(
+            hidden[s], down_ref[:, lanes_of(i)], preferred_element_type=F32
+        ).astype(BF16)
+
+    def send_result(i, s):
+        res[i, s] = down_rows(i, s)
+        remote(res.at[i, s], ret.at[i, g], r_send, r_recv.at[i], s, t).start()
+
+    order = near + far
+
+    def expert_order(j):
+        return sum(jnp.where(j == n, p, 0) for n, p in enumerate(order))
+
+    lax.fori_loop(0, ep - 1, expert_step, 0)
+
+    def down_step(i, carry):
+        for p in far:
+            send_result(i, partner(g, p, ep))
+
+        @pl.when(i < chunks - half)
+        def _():
+            for p in near:
+                send_result(i + half, partner(g, p, ep))
+
+        return carry
+
+    lax.fori_loop(0, chunks, down_step, 0)
+    activate(g)
+
+    def own_step(i, carry):
+        ret[i, g] = down_rows(i, g)
+        return carry
+
+    lax.fori_loop(0, chunks, own_step, 0)
+    spread[...] = spread_t[...].T.astype(BF16)
     normalise(lambda k, at: whole[k, at, :], rows)
     contract = (((1,), (1,)), ((), ()))
     sg = lax.dot_general(norm[...], sgate_ref[...], contract, preferred_element_type=F32)
     su = lax.dot_general(norm[...], sup_ref[...], contract, preferred_element_type=F32)
     shidden[...] = (jax.nn.silu(sg) * su).astype(BF16)
 
-    for load in loads[5:]:
-        load.wait()
-
-    def expert_step(p, carry):
-        s = partner(g, p, ep)
-
-        @pl.when(p > 0)
-        def _():
-            remote(sent.at[:, s], inc.at[:, s], b_send, b_recv.at[s], s, t).wait_recv()
-
-        normalise(lambda k, at: inc[k, s, at, :], slots)
-        got = norm[0:slots, :]
-        gate_act = jnp.dot(got, gate_ref[...], preferred_element_type=F32)
-        up_act = jnp.dot(got, up_ref[...], preferred_element_type=F32)
-        hidden[s] = (jax.nn.silu(gate_act) * up_act).astype(BF16)
-
-        @pl.when(p == 0)
-        def _():
-            def own_step(i, carry):
-                ret[i, g] = down_rows(i, g)
-                return carry
-
-            lax.fori_loop(0, chunks, own_step, 0)
-
-        is_near = functools.reduce(jnp.logical_or, [p == n for n in near])
-
-        @pl.when(is_near)
-        def _():
-            def near_step(i, carry):
-                send_result(i, s)
-                return carry
-
-            lax.fori_loop(0, half, near_step, 0)
-
-        return carry
-
-    def lanes_of(i):
-        return pl.ds(pl.multiple_of(i * cols, cols), cols)
-
-    def down_rows(i, s):
-        return jnp.dot(
-            hidden[s], down_ref[:, lanes_of(i)], preferred_element_type=F32
-        ).astype(BF16)
-
-    def send_result(i, s):
-        res[i, s] = down_rows(i, s)
-        remote(res.at[i, s], ret.at[i, g], r_send, r_recv.at[i], s, t).start()
-
-    lax.fori_loop(0, ep, expert_step, 0)
-
-    def down_step(i, carry):
-        for p in far:
-            send_result(i, partner(g, p, ep))
-
-        @pl.when(i < chunks - half)
-        def _():
-            for p in near:
-                send_result(i + half, partner(g, p, ep))
-
-        return carry
-
-    lax.fori_loop(0, chunks, down_step, 0)
 
     def pair_copy(i):
         return remote(pair_out.at[i], pair_in.at[i], p_send, p_recv.at[i], g, mate)
@@ -400,7 +516,10 @@
     lax.fori_loop(0, chunks, out_step, 0)
 
     others = pl.ds(0, ep - 1)
-    remote(sent.at[:, others], inc.at[:, others], b_send, b_recv.at[g], g, mate).wait_send()
+    over = pl.ds(0, crossed)
+    remote(
+        sent.at[:, others, over], inc.at[:, others, over], b_send, b_recv.at[g], g, mate
+    ).wait_send()
     remote(res.at[:, others], ret.at[:, others], r_send, r_recv.at[0], g, mate).wait_send()
     remote(pair_out, pair_in, p_send, p_recv.at[0], g, mate).wait_send()
 
@@ -416,9 +535,24 @@
         def _():
             downward(k).wait_send()
 
+        if not shift:
+            return carry
+        extra_forward(k).wait_send()
+
+        @pl.when((chip <= z) & (z < chips - 1))
+        def _():
+            extra_upward(k).wait_send()
+
+        @pl.when((chip >= z) & (z > 0))
+        def _():
+            extra_downward(k).wait_send()
+
         return carry
 
     lax.fori_loop(0, chips, sent_step, 0)
+    if shift:
+        remote(ids_other, ids_other, i_send, i_recv, g, mate).wait_send()
+        remote(extra.at[t], extra.at[t], x_send, x_recv, g, mate).wait_send()
 
 
 def on_device(
@@ -448,12 +582,17 @@
     cols = 256
     chunks = width // cols
     chips = tp // 2
+    shift = max(1, tp // 8)
+    fits = (ep & (ep - 1)) == 0 and ep > 1 and slot_cap % 8 == 0 and block % 8 == 0
+    if not fits or shift * block > 128 or rows < 128 or feat != cols:
+        shift = 0
+    lanes = min(rows, 128)
 
     vmem = pl.BlockSpec(memory_space=pltpu.VMEM)
     anywhere = pl.BlockSpec(memory_space=pl.ANY)
     dma = pltpu.SemaphoreType.DMA
     return pl.pallas_call(
-        functools.partial(layer_kernel, (ep, tp, rows, slots, slot_cap, feat, chunks, cols)),
+        functools.partial(layer_kernel, (ep, tp, rows, slots, slot_cap, feat, chunks, cols, shift)),
         out_shape=jax.ShapeDtypeStruct((block, width), BF16),
         in_specs=[anywhere] * 11,
         out_specs=vmem,
@@ -479,6 +618,9 @@
             pltpu.VMEM((rows, shared_rows), BF16),
             pltpu.VMEM((chunks, ep, slots, cols), BF16),
             pltpu.VMEM((chunks, ep, slots, cols), BF16),
+            pltpu.VMEM((ep - 1, top_count, lanes), jnp.int32),
+            pltpu.VMEM((tp, ep - 1, max(8, shift * block), feat), BF16),
+            pltpu.VMEM((ep - 1, max(8, shift * slot_cap), lanes), BF16),
             pltpu.VMEM((2, tp, block, cols), F32),
             pltpu.VMEM((chunks, block, cols), F32),
             pltpu.VMEM((chunks, chips, block, cols), BF16),
@@ -499,6 +641,14 @@
             dma((chunks,)),
             dma,
             dma,
+            dma,
+            dma,
+            dma,
+            dma,
+            dma((chips,)),
+            dma((chips,)),
+            dma((chips,)),
+            dma((tp,)),
         ],
         compiler_params=pltpu.CompilerParams(
             collective_id=0, has_side_effects=True, vmem_limit_bytes=56 * 1024 * 1024

time: 88.3 us -> 85.3 us (0.966)
  Pallas kernels: 86.4 us -> 83.4 us
    pallas_call x1, Pallas kernels: 86.4 us -> 83.4 us  [on_device(): pl.pallas_call(functools.partial(layer_kernel, (ep, tp, rows, slots, slot...]
where the time goes in v3:
time: 85.3 us; the launch traced here: 85.1 us
  Pallas kernels  83.4 us (98%)
  local copies, waits for them, and re-layouts  1.67 us (2%)
    pallas_call x1, Pallas kernels, on_device(): pl.pallas_call(functools.partial(layer_kernel, (ep, tp, rows, slots, slot...  83.4 us

profile of v3, /device:TPU:0, one launch (start us, length us, event | category | flops | bytes accessed | tf_op | source)
XLA Modules:
  0.0 85.1 jit_solution(17626741072064067979)
XLA Ops:
  0.0 83.4 %moe_layer.1 = bf16[64,2048]{1,0:T(8,128)(2,1)} custom-call(bf16[512,256]{1,0:T(8,128)(2,1)} %tokens_hbm.1, s32[6,512]{1,0:T(8,128)} %bitcast.10, f32[6,512]{1,0:T(8,128)} %bitcast.11, f32[1,2048]{1,0:T(1,128)} %bitcast.12, f32[1,2048]{1,0:T(1,128)} %bitcast.13, bf16[64,2048]{1,0:T(8,128)(2,1)} %sgate_hbm.1, bf16[64,2048]{1,0:T(8,128)(2,1)} %sup_hbm.1, ...), custom_call_target="tpu_custom_call" | custom-call | tf_op jit(solution)/shard_map/moe_layer/pallas_call | solution.py:594
  83.4 1.7 %copy.13 = bf16[64,2048]{1,0:T(8,128)(2,1)} copy(bf16[64,2048]{1,0:T(8,128)(2,1)} %moe_layer.1) | data formatting | bytes 524288

commit v4 on v3

--- a/solution.py
+++ b/solution.py
@@ -257,7 +257,7 @@
 
     near = [p for p in range(1, ep) if not p & (p - 1)]
     far = [p for p in range(1, ep) if p & (p - 1)]
-    half = chunks // 8
+    half = chunks * 1 // 8
 
     def send_rows(k, p):
         e = partner(g, p, ep)
@@ -427,40 +427,39 @@
         res[i, s] = down_rows(i, s)
         remote(res.at[i, s], ret.at[i, g], r_send, r_recv.at[i], s, t).start()
 
-    order = near + far
-
-    def expert_order(j):
-        return sum(jnp.where(j == n, p, 0) for n, p in enumerate(order))
-
-    lax.fori_loop(0, ep - 1, expert_step, 0)
-
-    def down_step(i, carry):
-        for p in far:
-            send_result(i, partner(g, p, ep))
-
-        @pl.when(i < chunks - half)
-        def _():
-            for p in near:
-                send_result(i + half, partner(g, p, ep))
-
-        return carry
-
-    lax.fori_loop(0, chunks, down_step, 0)
-    activate(g)
-
-    def own_step(i, carry):
-        ret[i, g] = down_rows(i, g)
-        return carry
-
-    lax.fori_loop(0, chunks, own_step, 0)
-    spread[...] = spread_t[...].T.astype(BF16)
     normalise(lambda k, at: whole[k, at, :], rows)
     contract = (((1,), (1,)), ((), ()))
     sg = lax.dot_general(norm[...], sgate_ref[...], contract, preferred_element_type=F32)
     su = lax.dot_general(norm[...], sup_ref[...], contract, preferred_element_type=F32)
     shidden[...] = (jax.nn.silu(sg) * su).astype(BF16)
 
-
+    spread[...] = spread_t[...].T.astype(BF16)
+    order = near + far
+
+    def expert_order(j):
+        return sum(jnp.where(j == n, p, 0) for n, p in enumerate(order))
+
+    lax.fori_loop(0, ep - 1, expert_step, 0)
+
+    def down_step(i, carry):
+        for p in far:
+            send_result(i, partner(g, p, ep))
+
+        @pl.when(i < chunks - half)
+        def _():
+            for p in near:
+                send_result(i + half, partner(g, p, ep))
+
+        return carry
+
+    lax.fori_loop(0, chunks, down_step, 0)
+    activate(g)
+
+    def own_step(i, carry):
+        ret[i, g] = down_rows(i, g)
+        return carry
+
+    lax.fori_loop(0, chunks, own_step, 0)
     def pair_copy(i):
         return remote(pair_out.at[i], pair_in.at[i], p_send, p_recv.at[i], g, mate)
 
@@ -491,17 +490,11 @@
         own[i] = part[i % 2, t] + pair_in[i, z].astype(F32)
 
     def sum_step(i, carry):
-        @pl.when(i < chunks)
-        def _():
-            produce(i)
-
-        @pl.when(i > 0)
-        def _():
-            finish(i - 1)
-
+        produce(i)
+        finish(i)
         return carry
 
-    lax.fori_loop(0, chunks + 1, sum_step, 0)
+    lax.fori_loop(0, chunks, sum_step, 0)
 
     rest = pl.ds(0, chips - 1)
     remote(far_out.at[:, rest], far_in.at[:, rest], q_send, q_recv, g, mate).wait()
@@ -593,7 +586,7 @@
     dma = pltpu.SemaphoreType.DMA
     return pl.pallas_call(
         functools.partial(layer_kernel, (ep, tp, rows, slots, slot_cap, feat, chunks, cols, shift)),
-        out_shape=jax.ShapeDtypeStruct((block, width), BF16),
+        out_shape=pltpu.VMEM((block, width), BF16),
         in_specs=[anywhere] * 11,
         out_specs=vmem,
         scratch_shapes=[

time: 85.3 us -> 82 us (0.961)
  Pallas kernels: 83.4 us -> 81 us
  local copies, waits for them, and re-layouts: 1.67 us -> 0.71 us
    pallas_call x1, Pallas kernels: 83.4 us -> 81 us  [on_device(): pl.pallas_call(functools.partial(layer_kernel, (ep, tp, rows, slots, slot...]
    unnamed x1, local copies, waits for them, and re-layouts: 1.67 us -> 0.71 us
where the time goes in v4:
time: 82 us; the launch traced here: 81.7 us
  Pallas kernels  81 us (99%)
    pallas_call x1, Pallas kernels, on_device(): pl.pallas_call(functools.partial(layer_kernel, (ep, tp, rows, slots, slot...  81 us

profile of v4, /device:TPU:0, one launch (start us, length us, event | category | flops | bytes accessed | tf_op | source)
XLA Modules:
  0.0 81.7 jit_solution(3080065799934606010)
XLA Ops:
  0.0 81.0 %moe_layer.1 = bf16[64,2048]{1,0:T(8,128)(2,1)S(1)} custom-call(bf16[512,256]{1,0:T(8,128)(2,1)} %tokens_hbm.1, s32[6,512]{1,0:T(8,128)} %bitcast.10, f32[6,512]{1,0:T(8,128)} %bitcast.11, f32[1,2048]{1,0:T(1,128)} %bitcast.12, f32[1,2048]{1,0:T(1,128)} %bitcast.13, bf16[64,2048]{1,0:T(8,128)(2,1)} %sgate_hbm.1, bf16[64,2048]{1,0:T(8,128)(2,1)} %sup_hbm.1, ...), custom_call_target="tpu_custom_call" | custom-call | tf_op jit(solution)/shard_map/moe_layer/pallas_call | solution.py:587
  81.0 0.7 copy.13

commit v5 on v4

--- a/solution.py
+++ b/solution.py
@@ -63,12 +63,23 @@
     ids_other,
     extra,
     pick_other,
+    affinity_other,
+    turn_weight,
+    turn_hidden,
+    mine,
+    t_out,
+    t_in,
+    line_out,
+    line_in,
+    y_out,
+    y_in,
     part,
     own,
     pair_out,
     pair_in,
     far_out,
     far_in,
+    relay,
     load_sem,
     first_sem,
     u_send,
@@ -83,6 +94,8 @@
     p_recv,
     q_send,
     q_recv,
+    o_send,
+    o_recv,
     i_send,
     i_recv,
     x_send,
@@ -91,8 +104,17 @@
     ed_send,
     ef_send,
     e_recv,
+    w_send,
+    w_recv,
+    t_send,
+    t_recv,
+    l_send,
+    l_recv,
+    y_send,
+    y_recv,
 ):
-    ep, tp, rows, slots, slot_cap, feat, chunks, cols, shift = sizes
+    ep, tp, rows, slots, slot_cap, feat, chunks, cols, shift, turn = sizes
+    paired = tp == 8 and turn > 0
     chips = tp // 2
     g = lax.axis_index("ep")
     t = lax.axis_index("tp")
@@ -164,6 +186,18 @@
         weight = jnp.sum(jnp.where(hits[e], weights, 0.0), axis=0, keepdims=True)
         pick[e] = jnp.where(line == place, 1.0, 0.0).astype(BF16)
         spread_t[pl.ds(e * slots, slots), :] = jnp.where(line == place, weight, 0.0)
+    returned = slots - turn * slot_cap
+    turn_rows = turn * block
+    turn_slots = turn * slot_cap
+    if turn:
+        turn_weight[...] = jnp.zeros(turn_weight.shape, BF16)
+
+        def clear_step(i, carry):
+            for e in range(ep):
+                ret[i, e, returned:slots, :] = jnp.zeros((turn_slots, cols), BF16)
+            return carry
+
+        lax.fori_loop(0, chunks, clear_step, 0)
     pl.semaphore_wait(barrier, len(partners))
 
     def forward(k):
@@ -197,6 +231,11 @@
         e = partner(g, p, ep)
         return remote(ids_ref.at[:, lanes], ids_other.at[p - 1], i_send, i_recv, e, t)
 
+    def affinity_copy(p):
+        lanes = pl.ds(0, ids_other.shape[2])
+        e = partner(g, p, ep)
+        return remote(affinity_ref.at[:, lanes], affinity_other.at[p - 1], w_send, w_recv, e, t)
+
     def extra_copy(p):
         e = partner(g, p, ep)
         rows_out = whole.at[t, pl.ds(0, extra_rows)]
@@ -217,6 +256,8 @@
         for p in range(1, ep):
             ids_copy(p).start()
             extra_copy(p).start()
+            if turn:
+                affinity_copy(p).start()
 
     def extra_onward(chip):
         k = chip * 2 + c
@@ -254,10 +295,23 @@
             named = (chosen[p] > 0.5) & (blocks < shift)
             place = jnp.where(named, base + ranks[p : p + 1, :], -1)
             pick_other[p] = jnp.where(line == place, 1.0, 0.0).astype(BF16)
+        if not turn:
+            return
+        remote(affinity_other, affinity_other, w_send, w_recv, g, mate).wait_recv()
+        base = (turn - 1 - blocks) * slot_cap
+        line = lax.broadcasted_iota(jnp.int32, ((ep - 1) * turn_slots, lanes), 0)
+        for p in range(ep - 1):
+            share = affinity_other[p] / jnp.sum(affinity_other[p], axis=0, keepdims=True)
+            hit = ids_other[p] == g * tp + t
+            weight = jnp.sum(jnp.where(hit, share * ROUTED_SCALE, 0.0), axis=0, keepdims=True)
+            named = (chosen[p] > 0.5) & (blocks < turn)
+            place = jnp.where(named, p * turn_slots + base + ranks[p : p + 1, :], -1)
+            spread_p = jnp.where(line == place, weight, 0.0).T.astype(BF16)
+            turn_weight[p * turn_rows : (p + 1) * turn_rows, :] = spread_p[:turn_rows, :]
 
     near = [p for p in range(1, ep) if not p & (p - 1)]
     far = [p for p in range(1, ep) if p & (p - 1)]
-    half = chunks * 1 // 8
+    half = chunks // 8
 
     def send_rows(k, p):
         e = partner(g, p, ep)
@@ -415,6 +469,9 @@
 
         return carry
 
+    def chunk_of(i):
+        return lax.rem(i + (2 - 2 * (z // 2)) * 2, chunks) if turn else i
+
     def lanes_of(i):
         return pl.ds(pl.multiple_of(i * cols, cols), cols)
 
@@ -424,8 +481,23 @@
         ).astype(BF16)
 
     def send_result(i, s):
-        res[i, s] = down_rows(i, s)
-        remote(res.at[i, s], ret.at[i, g], r_send, r_recv.at[i], s, t).start()
+        n = chunk_of(i)
+        res[n, s] = down_rows(n, s)
+
+        @pl.when(i < held)
+        def _():
+            result_copy(n, s).start()
+
+    def result_copy(n, s):
+        back = pl.ds(0, returned)
+        return remote(res.at[n, s, back], ret.at[n, g, back], r_send, r_recv.at[n], s, t)
+
+    held = chunks * 6 // 8 if turn else chunks
+
+    def held_step(i, carry):
+        for p in far + near:
+            result_copy(chunk_of(i), partner(g, p, ep)).start()
+        return carry
 
     normalise(lambda k, at: whole[k, at, :], rows)
     contract = (((1,), (1,)), ((), ()))
@@ -441,6 +513,52 @@
 
     lax.fori_loop(0, ep - 1, expert_step, 0)
 
+    def turned_copy(i):
+        return remote(t_out.at[i], t_in.at[i], t_send, t_recv, g, mate)
+
+    def turned_back(p):
+        return remote(y_out.at[p - 1], y_in.at[p - 1], y_send, y_recv, partner(g, p, ep), t)
+
+    def turned_rows(i):
+        result = jnp.dot(
+            turn_hidden[...], down_ref[:, lanes_of(i)], preferred_element_type=F32
+        ).astype(BF16)
+        return jnp.dot(turn_weight[...], result, preferred_element_type=F32)
+
+    def turn_start():
+        for p in range(1, ep):
+            at = slice((p - 1) * turn_slots, p * turn_slots)
+            turn_hidden[at, :] = hidden[partner(g, p, ep), returned:slots, :]
+
+    def turn_step(i):
+        t_out[i] = turned_rows(i * 2 + 1 - c).astype(BF16)
+        turned_copy(i).start()
+        mine[i] = turned_rows(i * 2 + c)
+
+    def line_start():
+        remote(t_out, t_in, t_send, t_recv, g, mate).wait_recv()
+
+        def add_step(j, carry):
+            mine[j] = mine[j] + t_in[j].astype(F32)
+            return carry
+
+        lax.fori_loop(0, chips, add_step, 0)
+
+        for d in range(1, chips):
+            zz = partner(z, d, chips)
+            line_out[zz] = mine[zz].astype(BF16)
+            remote(line_out.at[zz], line_in.at[z], l_send, l_recv, g, zz * 2 + c).start()
+
+    def line_finish():
+        some = pl.ds(0, chips - 1)
+        remote(line_out.at[some], line_in.at[some], l_send, l_recv, g, mate).wait_recv()
+        total = mine[z]
+        for d in range(1, chips):
+            total = total + line_in[partner(z, d, chips)].astype(F32)
+        for p in range(1, ep):
+            y_out[p - 1] = total[(p - 1) * turn_rows : p * turn_rows, :].astype(BF16)
+            turned_back(p).start()
+
     def down_step(i, carry):
         for p in far:
             send_result(i, partner(g, p, ep))
@@ -450,8 +568,20 @@
             for p in near:
                 send_result(i + half, partner(g, p, ep))
 
+        if turn:
+
+            @pl.when(i < chips)
+            def _():
+                turn_step(i)
+
+            @pl.when(i == chips + 1)
+            def _():
+                line_start()
+
         return carry
 
+    if turn:
+        turn_start()
     lax.fori_loop(0, chunks, down_step, 0)
     activate(g)
 
@@ -460,60 +590,154 @@
         return carry
 
     lax.fori_loop(0, chunks, own_step, 0)
-    def pair_copy(i):
-        return remote(pair_out.at[i], pair_in.at[i], p_send, p_recv.at[i], g, mate)
-
-    def produce(i):
+    def pair_copy(n):
+        return remote(pair_out.at[n], pair_in.at[n], p_send, p_recv.at[n], g, mate)
+
+    def produce(i, n):
         others = pl.ds(0, ep - 1)
-        remote(res.at[i, others], ret.at[i, others], r_send, r_recv.at[i], g, mate).wait_recv()
+        back = pl.ds(0, returned)
+        came = remote(res.at[n, others, back], ret.at[n, others, back], r_send, r_recv.at[n], g, mate)
+        came.wait_recv()
         total = jnp.dot(
-            spread[...], ret[i].reshape(ep * slots, cols), preferred_element_type=F32
-        ) + jnp.dot(shidden[...], sdown_ref[:, lanes_of(i)], preferred_element_type=F32)
+            spread[...], ret[n].reshape(ep * slots, cols), preferred_element_type=F32
+        ) + jnp.dot(shidden[...], sdown_ref[:, lanes_of(n)], preferred_element_type=F32)
         part[i % 2] = total.reshape(part.shape[1:])
+        if turn:
+
+            @pl.when(n == t)
+            def _():
+                remote(y_out, y_in, y_send, y_recv, g, mate).wait_recv()
+                more = y_in[0].astype(F32)
+                for p in range(1, ep - 1):
+                    more = more + y_in[p].astype(F32)
+                more = more.reshape((turn,) + part.shape[2:])
+                part[i % 2, 0:turn] = part[i % 2, 0:turn] + more
+
         for zz in range(chips):
-            pair_out[i, zz] = part[i % 2, zz * 2 + 1 - c].astype(BF16)
-        pair_copy(i).start()
-
-    def finish(i):
-        pair_copy(i).wait_recv()
+            pair_out[n, zz] = part[i % 2, zz * 2 + 1 - c].astype(BF16)
+        pair_copy(n).start()
+
+    inner = (z == 1) | (z == 2)
+    beside = partner(z, 1, chips)
+    across = (2 - 2 * (z // 2)) if paired else 0
+    relayed = chunks - 4
+
+    def mixed(i, n, zz):
+        return part[i % 2, zz * 2 + c] + pair_in[n, zz].astype(F32)
+
+    def far_copy(n, zz, send):
+        return remote(far_out.at[n, zz], far_in.at[n, z], send, q_recv.at[n], g, zz * 2 + c)
+
+    def relay_copy(n):
+        two = pl.ds(across, 2)
+        return remote(far_out.at[n, two], relay.at[n], o_send, o_recv.at[n], g, beside * 2 + c)
+
+    def finish(i, n):
+        pair_copy(n).wait_recv()
+        direct = (i >= relayed) if paired else True
         for d in range(1, chips):
             zz = partner(z, d, chips)
-            far_out[i, zz] = (part[i % 2, zz * 2 + c] + pair_in[i, zz].astype(F32)).astype(BF16)
-            remote(
-                far_out.at[i, zz],
-                far_in.at[i, z],
-                q_send,
-                q_recv,
-                g,
-                zz * 2 + c,
-            ).start()
-        own[i] = part[i % 2, t] + pair_in[i, z].astype(F32)
+            far_out[n, zz] = mixed(i, n, zz).astype(BF16)
+            if d == 1 or not paired:
+                far_copy(n, zz, q_send).start()
+        if paired:
+
+            for send, which in ((q_send, inner), (o_send, jnp.logical_not(inner))):
+
+                @pl.when(direct & which)
+                def _():
+                    for k in range(2):
+                        far_copy(n, across + k, send).start()
+
+            @pl.when(jnp.logical_not(direct | inner))
+            def _():
+                relay_copy(n).start()
+
+        own[n] = part[i % 2, t] + pair_in[n, z].astype(F32)
+
+    def pass_on(i, n):
+        relay_copy(n).wait_recv()
+        for k in range(2):
+            zz = across + k
+            far_out[n, zz] = (mixed(i, n, zz) + relay[n, k].astype(F32)).astype(BF16)
+            far_copy(n, zz, q_send).start()
 
     def sum_step(i, carry):
-        produce(i)
-        finish(i)
+        n = chunk_of(i)
+        produce(i, n)
+        if paired:
+
+            @pl.when(inner & (i > 0) & (i <= relayed))
+            def _():
+                pass_on(i - 1, chunk_of(i - 1))
+
+        finish(i, n)
+        if turn:
+
+            @pl.when(i == 1)
+            def _():
+                line_finish()
+                lax.fori_loop(held, chunks, held_step, 0)
+
         return carry
 
     lax.fori_loop(0, chunks, sum_step, 0)
 
+    def gathered(n, count):
+        some = pl.ds(0, count)
+        return remote(far_out.at[n, some], far_in.at[n, some], q_send, q_recv.at[n], g, mate)
+
+    def put(n, sources):
+        gathered(n, len(sources)).wait_recv()
+        total = own[n]
+        for source in sources:
+            total = total + far_in[n, source].astype(F32)
+        out_ref[:, lanes_of(n)] = total.astype(BF16)
+
+    def out_step(i, carry):
+        n = chunk_of(i)
+        if not paired:
+            put(n, [partner(z, d, chips) for d in range(1, chips)])
+            return carry
+        straight = lax.rem(n + chunks - z // 2 * 4, chunks) >= relayed
+
+        @pl.when(straight)
+        def _():
+            put(n, [beside, across, across + 1])
+
+        @pl.when(jnp.logical_not(straight))
+        def _():
+            put(n, [beside, 2 - z // 2])
+
+        return carry
+
+    lax.fori_loop(0, chunks, out_step, 0)
+
     rest = pl.ds(0, chips - 1)
-    remote(far_out.at[:, rest], far_in.at[:, rest], q_send, q_recv, g, mate).wait()
-
-    def out_step(i, carry):
-        total = own[i]
-        for d in range(1, chips):
-            total = total + far_in[i, partner(z, d, chips)].astype(F32)
-        out_ref[:, lanes_of(i)] = total.astype(BF16)
-        return carry
-
-    lax.fori_loop(0, chunks, out_step, 0)
+    if paired:
+
+        @pl.when(inner)
+        def _():
+            remote(far_out.at[:, rest], far_in.at[:, rest], q_send, q_recv.at[0], g, mate).wait_send()
+
+        @pl.when(jnp.logical_not(inner))
+        def _():
+            one = pl.ds(0, 1)
+            remote(far_out.at[:, one], far_in.at[:, one], q_send, q_recv.at[0], g, mate).wait_send()
+            remote(relay, relay, o_send, o_recv.at[0], g, mate).wait_send()
+
+    else:
+        remote(far_out.at[:, rest], far_in.at[:, rest], q_send, q_recv.at[0], g, mate).wait_send()
 
     others = pl.ds(0, ep - 1)
     over = pl.ds(0, crossed)
     remote(
         sent.at[:, others, over], inc.at[:, others, over], b_send, b_recv.at[g], g, mate
     ).wait_send()
-    remote(res.at[:, others], ret.at[:, others], r_send, r_recv.at[0], g, mate).wait_send()
+    back = pl.ds(0, returned)
+    remote(
+        res.at[:, others, back], ret.at[:, others, back], r_send, r_recv.at[0], g, mate
+    ).wait_send()
     remote(pair_out, pair_in, p_send, p_recv.at[0], g, mate).wait_send()
 
     def sent_step(chip, carry):
@@ -546,6 +770,14 @@
     if shift:
         remote(ids_other, ids_other, i_send, i_recv, g, mate).wait_send()
         remote(extra.at[t], extra.at[t], x_send, x_recv, g, mate).wait_send()
+    if not turn:
+        return
+    remote(affinity_other, affinity_other, w_send, w_recv, g, mate).wait_send()
+    remote(t_out, t_in, t_send, t_recv, g, mate).wait_send()
+    remote(y_out, y_in, y_send, y_recv, g, mate).wait_send()
+
+    some = pl.ds(0, chips - 1)
+    remote(line_out.at[some], line_in.at[some], l_send, l_recv, g, mate).wait_send()
 
 
 def on_device(
@@ -580,12 +812,16 @@
     if not fits or shift * block > 128 or rows < 128 or feat != cols:
         shift = 0
     lanes = min(rows, 128)
+    turn = 1 * shift if 1 * shift * block <= 128 and chunks == tp and chips > 2 else 0
+    turn_rows = max(8, (ep - 1) * turn * block)
+    turn_slots = max(8, (ep - 1) * turn * slot_cap)
+    line = (chips if turn else 1, turn_rows, cols)
 
     vmem = pl.BlockSpec(memory_space=pltpu.VMEM)
     anywhere = pl.BlockSpec(memory_space=pl.ANY)
     dma = pltpu.SemaphoreType.DMA
     return pl.pallas_call(
-        functools.partial(layer_kernel, (ep, tp, rows, slots, slot_cap, feat, chunks, cols, shift)),
+        functools.partial(layer_kernel, (ep, tp, rows, slots, slot_cap, feat, chunks, cols, shift, turn)),
         out_shape=pltpu.VMEM((block, width), BF16),
         in_specs=[anywhere] * 11,
         out_specs=vmem,
@@ -614,12 +850,23 @@
             pltpu.VMEM((ep - 1, top_count, lanes), jnp.int32),
             pltpu.VMEM((tp, ep - 1, max(8, shift * block), feat), BF16),
             pltpu.VMEM((ep - 1, max(8, shift * slot_cap), lanes), BF16),
+            pltpu.VMEM((ep - 1, top_count, lanes), F32),
+            pltpu.VMEM((turn_rows, turn_slots), BF16),
+            pltpu.VMEM((turn_slots, hid), BF16),
+            pltpu.VMEM(line, F32),
+            pltpu.VMEM(line, BF16),
+            pltpu.VMEM(line, BF16),
+            pltpu.VMEM(line, BF16),
+            pltpu.VMEM(line, BF16),
+            pltpu.VMEM((ep - 1, max(8, turn * block), cols), BF16),
+            pltpu.VMEM((ep - 1, max(8, turn * block), cols), BF16),
             pltpu.VMEM((2, tp, block, cols), F32),
             pltpu.VMEM((chunks, block, cols), F32),
             pltpu.VMEM((chunks, chips, block, cols), BF16),
             pltpu.VMEM((chunks, chips, block, cols), BF16),
             pltpu.VMEM((chunks, chips, block, cols), BF16),
             pltpu.VMEM((chunks, chips, block, cols), BF16),
+            pltpu.VMEM((chunks, 2, block, cols), BF16),
             dma((8,)),
             dma((3,)),
             dma((chips,)),
@@ -633,7 +880,9 @@
             dma,
             dma((chunks,)),
             dma,
-            dma,
+            dma((chunks,)),
+            dma,
+            dma((chunks,)),
             dma,
             dma,
             dma,
@@ -642,6 +891,14 @@
             dma((chips,)),
             dma((chips,)),
             dma((tp,)),
+            dma,
+            dma,
+            dma,
+            dma,
+            dma,
+            dma,
+            dma,
+            dma,
         ],
         compiler_params=pltpu.CompilerParams(
             collective_id=0, has_side_effects=True, vmem_limit_bytes=56 * 1024 * 1024

time: 82 us -> 81.4 us (level)
  no operation moved by 1% of the time
where the time goes in v5:
time: 81.4 us; the launch traced here: 81.1 us
  Pallas kernels  80.4 us (99%)
    pallas_call x1, Pallas kernels, on_device(): pl.pallas_call(functools.partial(layer_kernel, (ep, tp, rows, slots, slot...  80.4 us

profile of v5, /device:TPU:0, one launch (start us, length us, event | category | flops | bytes accessed | tf_op | source)
XLA Modules:
  0.0 81.1 jit_solution(13444568790189444921)
XLA Ops:
  0.0 80.4 %moe_layer.1 = bf16[64,2048]{1,0:T(8,128)(2,1)S(1)} custom-call(bf16[512,256]{1,0:T(8,128)(2,1)} %tokens_hbm.1, s32[6,512]{1,0:T(8,128)} %bitcast.10, f32[6,512]{1,0:T(8,128)} %bitcast.11, f32[1,2048]{1,0:T(1,128)} %bitcast.12, f32[1,2048]{1,0:T(1,128)} %bitcast.13, bf16[64,2048]{1,0:T(8,128)(2,1)} %sgate_hbm.1, bf16[64,2048]{1,0:T(8,128)(2,1)} %sup_hbm.1, ...), custom_call_target="tpu_custom_call" | custom-call | tf_op jit(solution)/shard_map/moe_layer/pallas_call | solution.py:823
  80.4 0.7 copy.13

commit v6 on v5

--- a/solution.py
+++ b/solution.py
@@ -64,13 +64,13 @@
     extra,
     pick_other,
     affinity_other,
-    turn_weight,
-    turn_hidden,
+    spread_other,
     mine,
     t_out,
     t_in,
     line_out,
     line_in,
+    hop_in,
     y_out,
     y_in,
     part,
@@ -112,9 +112,12 @@
     l_recv,
     y_send,
     y_recv,
+    m_send,
+    m_recv,
+    h_send,
+    h_recv,
 ):
-    ep, tp, rows, slots, slot_cap, feat, chunks, cols, shift, turn = sizes
-    paired = tp == 8 and turn > 0
+    ep, tp, rows, slots, slot_cap, feat, chunks, cols, shift = sizes
     chips = tp // 2
     g = lax.axis_index("ep")
     t = lax.axis_index("tp")
@@ -186,18 +189,9 @@
         weight = jnp.sum(jnp.where(hits[e], weights, 0.0), axis=0, keepdims=True)
         pick[e] = jnp.where(line == place, 1.0, 0.0).astype(BF16)
         spread_t[pl.ds(e * slots, slots), :] = jnp.where(line == place, weight, 0.0)
-    returned = slots - turn * slot_cap
-    turn_rows = turn * block
-    turn_slots = turn * slot_cap
-    if turn:
-        turn_weight[...] = jnp.zeros(turn_weight.shape, BF16)
-
-        def clear_step(i, carry):
-            for e in range(ep):
-                ret[i, e, returned:slots, :] = jnp.zeros((turn_slots, cols), BF16)
-            return carry
-
-        lax.fori_loop(0, chunks, clear_step, 0)
+    sent_chunks = chunks - 1 if shift else chunks
+    if shift:
+        ret[chunks - 1] = jnp.zeros(ret.shape[1:], BF16)
     pl.semaphore_wait(barrier, len(partners))
 
     def forward(k):
@@ -227,14 +221,12 @@
     extra_rows = shift * block
 
     def ids_copy(p):
-        lanes = pl.ds(0, ids_other.shape[2])
         e = partner(g, p, ep)
-        return remote(ids_ref.at[:, lanes], ids_other.at[p - 1], i_send, i_recv, e, t)
+        return remote(ids_ref, ids_other.at[p - 1], i_send, i_recv, e, t)
 
     def affinity_copy(p):
-        lanes = pl.ds(0, ids_other.shape[2])
         e = partner(g, p, ep)
-        return remote(affinity_ref.at[:, lanes], affinity_other.at[p - 1], w_send, w_recv, e, t)
+        return remote(affinity_ref, affinity_other.at[p - 1], w_send, w_recv, e, t)
 
     def extra_copy(p):
         e = partner(g, p, ep)
@@ -254,9 +246,16 @@
 
     if shift:
         for p in range(1, ep):
-            ids_copy(p).start()
             extra_copy(p).start()
-            if turn:
+
+        @pl.when(c == 0)
+        def _():
+            for p in range(1, ep):
+                ids_copy(p).start()
+
+        @pl.when(c == 1)
+        def _():
+            for p in range(1, ep):
                 affinity_copy(p).start()
 
     def extra_onward(chip):
@@ -272,42 +271,46 @@
 
         extra_forward(k).start()
 
+    def ids_share():
+        return remote(ids_other, ids_other, m_send, m_recv, g, mate)
+
+    def affinity_share():
+        return remote(affinity_other, affinity_other, m_send, m_recv, g, mate)
+
     def pick_others():
-        remote(ids_other, ids_other, i_send, i_recv, g, mate).wait_recv()
-        lanes = ids_other.shape[2]
-        early = lax.broadcasted_iota(jnp.int32, (lanes, lanes), 0)
-        late = lax.broadcasted_iota(jnp.int32, (lanes, lanes), 1)
+        @pl.when(c == 0)
+        def _():
+            remote(ids_other, ids_other, i_send, i_recv, g, mate).wait_recv()
+            ids_share().start()
+            affinity_share().wait_recv()
+
+        @pl.when(c == 1)
+        def _():
+            remote(affinity_other, affinity_other, w_send, w_recv, g, mate).wait_recv()
+            affinity_share().start()
+            ids_share().wait_recv()
+
+        early = lax.broadcasted_iota(jnp.int32, (rows, rows), 0)
+        late = lax.broadcasted_iota(jnp.int32, (rows, rows), 1)
         before = jnp.where((early < late) & (early // block == late // block), 1.0, 0.0)
-        chosen = [
-            jnp.sum(jnp.where(ids_other[p] == g * tp + t, 1.0, 0.0), axis=0, keepdims=True)
-            for p in range(ep - 1)
-        ]
-        pad = [jnp.zeros((-(ep - 1) % 16, lanes), F32)]
+        hits = [ids_other[p] == g * tp + t for p in range(ep - 1)]
+        chosen = [jnp.sum(jnp.where(hit, 1.0, 0.0), axis=0, keepdims=True) for hit in hits]
+        pad = [jnp.zeros((-(ep - 1) % 16, rows), F32)]
         ranks = jnp.dot(
             jnp.concatenate(chosen + pad, axis=0).astype(BF16),
             before.astype(BF16),
             preferred_element_type=F32,
         ).astype(jnp.int32)
-        blocks = lax.broadcasted_iota(jnp.int32, (1, lanes), 1) // block
-        base = (shift - 1 - blocks) * slot_cap
-        line = lax.broadcasted_iota(jnp.int32, (shift * slot_cap, lanes), 0)
+        base = (tp - 1 - lax.broadcasted_iota(jnp.int32, (1, rows), 1) // block) * slot_cap
+        line = lax.broadcasted_iota(jnp.int32, (slots, rows), 0)
+        lanes = pick_other.shape[2]
+        late_line = lax.broadcasted_iota(jnp.int32, (shift * slot_cap, lanes), 0) + crossed
         for p in range(ep - 1):
-            named = (chosen[p] > 0.5) & (blocks < shift)
-            place = jnp.where(named, base + ranks[p : p + 1, :], -1)
-            pick_other[p] = jnp.where(line == place, 1.0, 0.0).astype(BF16)
-        if not turn:
-            return
-        remote(affinity_other, affinity_other, w_send, w_recv, g, mate).wait_recv()
-        base = (turn - 1 - blocks) * slot_cap
-        line = lax.broadcasted_iota(jnp.int32, ((ep - 1) * turn_slots, lanes), 0)
-        for p in range(ep - 1):
+            place = jnp.where(chosen[p] > 0.5, base + ranks[p : p + 1, :], -1)
+            pick_other[p] = jnp.where(late_line == place[:, :lanes], 1.0, 0.0).astype(BF16)
             share = affinity_other[p] / jnp.sum(affinity_other[p], axis=0, keepdims=True)
-            hit = ids_other[p] == g * tp + t
-            weight = jnp.sum(jnp.where(hit, share * ROUTED_SCALE, 0.0), axis=0, keepdims=True)
-            named = (chosen[p] > 0.5) & (blocks < turn)
-            place = jnp.where(named, p * turn_slots + base + ranks[p : p + 1, :], -1)
-            spread_p = jnp.where(line == place, weight, 0.0).T.astype(BF16)
-            turn_weight[p * turn_rows : (p + 1) * turn_rows, :] = spread_p[:turn_rows, :]
+            weight = jnp.sum(jnp.where(hits[p], share * ROUTED_SCALE, 0.0), axis=0, keepdims=True)
+            spread_other[p] = jnp.where(line == place, weight, 0.0).T.astype(BF16)
 
     near = [p for p in range(1, ep) if not p & (p - 1)]
     far = [p for p in range(1, ep) if p & (p - 1)]
@@ -469,9 +472,6 @@
 
         return carry
 
-    def chunk_of(i):
-        return lax.rem(i + (2 - 2 * (z // 2)) * 2, chunks) if turn else i
-
     def lanes_of(i):
         return pl.ds(pl.multiple_of(i * cols, cols), cols)
 
@@ -481,23 +481,8 @@
         ).astype(BF16)
 
     def send_result(i, s):
-        n = chunk_of(i)
-        res[n, s] = down_rows(n, s)
-
-        @pl.when(i < held)
-        def _():
-            result_copy(n, s).start()
-
-    def result_copy(n, s):
-        back = pl.ds(0, returned)
-        return remote(res.at[n, s, back], ret.at[n, g, back], r_send, r_recv.at[n], s, t)
-
-    held = chunks * 6 // 8 if turn else chunks
-
-    def held_step(i, carry):
-        for p in far + near:
-            result_copy(chunk_of(i), partner(g, p, ep)).start()
-        return carry
+        res[i, s] = down_rows(i, s)
+        remote(res.at[i, s], ret.at[i, g], r_send, r_recv.at[i], s, t).start()
 
     normalise(lambda k, at: whole[k, at, :], rows)
     contract = (((1,), (1,)), ((), ()))
@@ -513,76 +498,87 @@
 
     lax.fori_loop(0, ep - 1, expert_step, 0)
 
-    def turned_copy(i):
-        return remote(t_out.at[i], t_in.at[i], t_send, t_recv, g, mate)
-
-    def turned_back(p):
-        return remote(y_out.at[p - 1], y_in.at[p - 1], y_send, y_recv, partner(g, p, ep), t)
-
-    def turned_rows(i):
-        result = jnp.dot(
-            turn_hidden[...], down_ref[:, lanes_of(i)], preferred_element_type=F32
-        ).astype(BF16)
-        return jnp.dot(turn_weight[...], result, preferred_element_type=F32)
-
-    def turn_start():
-        for p in range(1, ep):
-            at = slice((p - 1) * turn_slots, p * turn_slots)
-            turn_hidden[at, :] = hidden[partner(g, p, ep), returned:slots, :]
-
-    def turn_step(i):
-        t_out[i] = turned_rows(i * 2 + 1 - c).astype(BF16)
-        turned_copy(i).start()
-        mine[i] = turned_rows(i * 2 + c)
+    def turn_step(p):
+        result = down_rows(chunks - 1, partner(g, p, ep))
+        total = jnp.dot(spread_other[p - 1], result, preferred_element_type=F32)
+        part[0] = total.reshape(part.shape[1:])
+        for zz in range(chips):
+            t_out[zz, p - 1] = part[0, zz * 2 + 1 - c].astype(BF16)
+            mine[zz, p - 1] = part[0, zz * 2 + c]
+
+        @pl.when(p == ep - 1)
+        def _():
+            remote(t_out, t_in, t_send, t_recv, g, mate).start()
+
+    paired = chips == 4 and shift > 0
+    inner = (z == 1) | (z == 2)
+    beside = partner(z, 1, chips)
+    across = 2 - 2 * (z // 2) if paired else 0
+
+    def line_copy(zz):
+        return remote(line_out.at[zz], line_in.at[z], l_send, l_recv, g, zz * 2 + c)
+
+    def hop_copy():
+        two = pl.ds(across, 2)
+        return remote(line_out.at[two], hop_in, h_send, h_recv, g, beside * 2 + c)
 
     def line_start():
         remote(t_out, t_in, t_send, t_recv, g, mate).wait_recv()
-
-        def add_step(j, carry):
-            mine[j] = mine[j] + t_in[j].astype(F32)
-            return carry
-
-        lax.fori_loop(0, chips, add_step, 0)
-
         for d in range(1, chips):
             zz = partner(z, d, chips)
-            line_out[zz] = mine[zz].astype(BF16)
-            remote(line_out.at[zz], line_in.at[z], l_send, l_recv, g, zz * 2 + c).start()
+            line_out[zz] = (mine[zz] + t_in[zz].astype(F32)).astype(BF16)
+            if d == 1 or not paired:
+                line_copy(zz).start()
+        if paired:
+
+            @pl.when(jnp.logical_not(inner))
+            def _():
+                hop_copy().start()
+
+    def line_pass():
+        hop_copy().wait_recv()
+        for k in range(2):
+            zz = across + k
+            total = mine[zz] + t_in[zz].astype(F32) + hop_in[k].astype(F32)
+            line_out[zz] = total.astype(BF16)
+            line_copy(zz).start()
 
     def line_finish():
-        some = pl.ds(0, chips - 1)
+        sources = [partner(z, d, chips) for d in range(1, chips)]
+        if paired:
+            sources = [beside, 2 - z // 2]
+        some = pl.ds(0, len(sources))
         remote(line_out.at[some], line_in.at[some], l_send, l_recv, g, mate).wait_recv()
-        total = mine[z]
-        for d in range(1, chips):
-            total = total + line_in[partner(z, d, chips)].astype(F32)
+        total = mine[z] + t_in[z].astype(F32)
+        for source in sources:
+            total = total + line_in[source].astype(F32)
+        y_out[...] = total.astype(BF16)
         for p in range(1, ep):
-            y_out[p - 1] = total[(p - 1) * turn_rows : p * turn_rows, :].astype(BF16)
-            turned_back(p).start()
+            there = partner(g, p, ep)
+            remote(y_out.at[p - 1], y_in.at[p - 1], y_send, y_recv, there, t).start()
 
     def down_step(i, carry):
         for p in far:
             send_result(i, partner(g, p, ep))
 
-        @pl.when(i < chunks - half)
+        @pl.when(i < sent_chunks - half)
         def _():
             for p in near:
                 send_result(i + half, partner(g, p, ep))
 
-        if turn:
-
-            @pl.when(i < chips)
-            def _():
-                turn_step(i)
-
-            @pl.when(i == chips + 1)
+        if shift:
+
+            @pl.when(i < ep - 1)
+            def _():
+                turn_step(i + 1)
+
+            @pl.when(i == ep + 1)
             def _():
                 line_start()
 
         return carry
 
-    if turn:
-        turn_start()
-    lax.fori_loop(0, chunks, down_step, 0)
+    lax.fori_loop(0, sent_chunks, down_step, 0)
     activate(g)
 
     def own_step(i, carry):
@@ -594,33 +590,21 @@
         return remote(pair_out.at[n], pair_in.at[n], p_send, p_recv.at[n], g, mate)
 
     def produce(i, n):
-        others = pl.ds(0, ep - 1)
-        back = pl.ds(0, returned)
-        came = remote(res.at[n, others, back], ret.at[n, others, back], r_send, r_recv.at[n], g, mate)
-        came.wait_recv()
+        @pl.when(n < sent_chunks)
+        def _():
+            others = pl.ds(0, ep - 1)
+            came = remote(res.at[n, others], ret.at[n, others], r_send, r_recv.at[n], g, mate)
+            came.wait_recv()
+
         total = jnp.dot(
             spread[...], ret[n].reshape(ep * slots, cols), preferred_element_type=F32
         ) + jnp.dot(shidden[...], sdown_ref[:, lanes_of(n)], preferred_element_type=F32)
         part[i % 2] = total.reshape(part.shape[1:])
-        if turn:
-
-            @pl.when(n == t)
-            def _():
-                remote(y_out, y_in, y_send, y_recv, g, mate).wait_recv()
-                more = y_in[0].astype(F32)
-                for p in range(1, ep - 1):
-                    more = more + y_in[p].astype(F32)
-                more = more.reshape((turn,) + part.shape[2:])
-                part[i % 2, 0:turn] = part[i % 2, 0:turn] + more
-
         for zz in range(chips):
             pair_out[n, zz] = part[i % 2, zz * 2 + 1 - c].astype(BF16)
         pair_copy(n).start()
 
-    inner = (z == 1) | (z == 2)
-    beside = partner(z, 1, chips)
-    across = (2 - 2 * (z // 2)) if paired else 0
-    relayed = chunks - 4
+    relayed = chunks - 3 if paired else 0
 
     def mixed(i, n, zz):
         return part[i % 2, zz * 2 + c] + pair_in[n, zz].astype(F32)
@@ -634,22 +618,20 @@
 
     def finish(i, n):
         pair_copy(n).wait_recv()
-        direct = (i >= relayed) if paired else True
         for d in range(1, chips):
             zz = partner(z, d, chips)
             far_out[n, zz] = mixed(i, n, zz).astype(BF16)
             if d == 1 or not paired:
                 far_copy(n, zz, q_send).start()
         if paired:
-
             for send, which in ((q_send, inner), (o_send, jnp.logical_not(inner))):
 
-                @pl.when(direct & which)
+                @pl.when((i >= relayed) & which)
                 def _():
                     for k in range(2):
                         far_copy(n, across + k, send).start()
 
-            @pl.when(jnp.logical_not(direct | inner))
+            @pl.when((i < relayed) & jnp.logical_not(inner))
             def _():
                 relay_copy(n).start()
 
@@ -662,6 +644,9 @@
             far_out[n, zz] = (mixed(i, n, zz) + relay[n, k].astype(F32)).astype(BF16)
             far_copy(n, zz, q_send).start()
 
+    def chunk_of(i):
+        return lax.rem(i + sent_chunks, chunks)
+
     def sum_step(i, carry):
         n = chunk_of(i)
         produce(i, n)
@@ -672,12 +657,17 @@
                 pass_on(i - 1, chunk_of(i - 1))
 
         finish(i, n)
-        if turn:
-
-            @pl.when(i == 1)
+        if shift:
+
+            if paired:
+
+                @pl.when(inner & (i == 0))
+                def _():
+                    line_pass()
+
+            @pl.when(i == 4)
             def _():
                 line_finish()
-                lax.fori_loop(held, chunks, held_step, 0)
 
         return carry
 
@@ -692,22 +682,36 @@
         total = own[n]
         for source in sources:
             total = total + far_in[n, source].astype(F32)
+        if shift:
+
+            @pl.when(n == sent_chunks)
+            def _():
+                remote(y_out, y_in, y_send, y_recv, g, mate).wait_recv()
+                more = y_in[0].astype(F32)
+                for p in range(1, ep - 1):
+                    more = more + y_in[p].astype(F32)
+                own[n] = total + more
+
+            @pl.when(n < sent_chunks)
+            def _():
+                own[n] = total
+
+            total = own[n]
         out_ref[:, lanes_of(n)] = total.astype(BF16)
 
     def out_step(i, carry):
-        n = chunk_of(i)
-        if not paired:
+        n = lax.rem(i, chunks)
+        later = lax.rem(n + chunks - sent_chunks, chunks) >= relayed
+
+        @pl.when(later)
+        def _():
             put(n, [partner(z, d, chips) for d in range(1, chips)])
-            return carry
-        straight = lax.rem(n + chunks - z // 2 * 4, chunks) >= relayed
-
-        @pl.when(straight)
-        def _():
-            put(n, [beside, across, across + 1])
-
-        @pl.when(jnp.logical_not(straight))
-        def _():
-            put(n, [beside, 2 - z // 2])
+
+        if paired:
+
+            @pl.when(jnp.logical_not(later))
+            def _():
+                put(n, [beside, 2 - z // 2])
 
         return carry
 
@@ -734,9 +738,9 @@
     remote(
         sent.at[:, others, over], inc.at[:, others, over], b_send, b_recv.at[g], g, mate
     ).wait_send()
-    back = pl.ds(0, returned)
+    some = pl.ds(0, sent_chunks)
     remote(
-        res.at[:, others, back], ret.at[:, others, back], r_send, r_recv.at[0], g, mate
+        res.at[some, others], ret.at[some, others], r_send, r_recv.at[0], g, mate
     ).wait_send()
     remote(pair_out, pair_in, p_send, p_recv.at[0], g, mate).wait_send()
 
@@ -768,16 +772,34 @@
 
     lax.fori_loop(0, chips, sent_step, 0)
     if shift:
-        remote(ids_other, ids_other, i_send, i_recv, g, mate).wait_send()
+
+        @pl.when(c == 0)
+        def _():
+            remote(ids_other, ids_other, i_send, i_recv, g, mate).wait_send()
+            ids_share().wait_send()
+
+        @pl.when(c == 1)
+        def _():
+            remote(affinity_other, affinity_other, w_send, w_recv, g, mate).wait_send()
+            affinity_share().wait_send()
+
         remote(extra.at[t], extra.at[t], x_send, x_recv, g, mate).wait_send()
-    if not turn:
-        return
-    remote(affinity_other, affinity_other, w_send, w_recv, g, mate).wait_send()
-    remote(t_out, t_in, t_send, t_recv, g, mate).wait_send()
-    remote(y_out, y_in, y_send, y_recv, g, mate).wait_send()
-
-    some = pl.ds(0, chips - 1)
-    remote(line_out.at[some], line_in.at[some], l_send, l_recv, g, mate).wait_send()
+        remote(t_out, t_in, t_send, t_recv, g, mate).wait_send()
+        remote(y_out, y_in, y_send, y_recv, g, mate).wait_send()
+        some = pl.ds(0, chips - 1)
+        if paired:
+
+            @pl.when(inner)
+            def _():
+                remote(line_out.at[some], line_in.at[some], l_send, l_recv, g, mate).wait_send()
+
+            @pl.when(jnp.logical_not(inner))
+            def _():
+                line_copy(beside).wait_send()
+                hop_copy().wait_send()
+
+        else:
+            remote(line_out.at[some], line_in.at[some], l_send, l_recv, g, mate).wait_send()
 
 
 def on_device(
@@ -809,19 +831,18 @@
     chips = tp // 2
     shift = max(1, tp // 8)
     fits = (ep & (ep - 1)) == 0 and ep > 1 and slot_cap % 8 == 0 and block % 8 == 0
-    if not fits or shift * block > 128 or rows < 128 or feat != cols:
+    if not fits or shift * block > 128 or rows < 128:
         shift = 0
     lanes = min(rows, 128)
-    turn = 1 * shift if 1 * shift * block <= 128 and chunks == tp and chips > 2 else 0
-    turn_rows = max(8, (ep - 1) * turn * block)
-    turn_slots = max(8, (ep - 1) * turn * slot_cap)
-    line = (chips if turn else 1, turn_rows, cols)
+    line = (chips, ep - 1, block, cols) if shift else (1, 1, 8, 128)
+    back = line[1:]
+    other = (ep - 1, rows, slots) if shift else (1, 8, 128)
 
     vmem = pl.BlockSpec(memory_space=pltpu.VMEM)
     anywhere = pl.BlockSpec(memory_space=pl.ANY)
     dma = pltpu.SemaphoreType.DMA
     return pl.pallas_call(
-        functools.partial(layer_kernel, (ep, tp, rows, slots, slot_cap, feat, chunks, cols, shift, turn)),
+        functools.partial(layer_kernel, (ep, tp, rows, slots, slot_cap, feat, chunks, cols, shift)),
         out_shape=pltpu.VMEM((block, width), BF16),
         in_specs=[anywhere] * 11,
         out_specs=vmem,
@@ -847,19 +868,19 @@
             pltpu.VMEM((rows, shared_rows), BF16),
             pltpu.VMEM((chunks, ep, slots, cols), BF16),
             pltpu.VMEM((chunks, ep, slots, cols), BF16),
-            pltpu.VMEM((ep - 1, top_count, lanes), jnp.int32),
+            pltpu.VMEM((ep - 1, top_count, rows), jnp.int32),
             pltpu.VMEM((tp, ep - 1, max(8, shift * block), feat), BF16),
             pltpu.VMEM((ep - 1, max(8, shift * slot_cap), lanes), BF16),
-            pltpu.VMEM((ep - 1, top_count, lanes), F32),
-            pltpu.VMEM((turn_rows, turn_slots), BF16),
-            pltpu.VMEM((turn_slots, hid), BF16),
+            pltpu.VMEM((ep - 1, top_count, rows), F32),
+            pltpu.VMEM(other, BF16),
             pltpu.VMEM(line, F32),
             pltpu.VMEM(line, BF16),
             pltpu.VMEM(line, BF16),
             pltpu.VMEM(line, BF16),
             pltpu.VMEM(line, BF16),
-            pltpu.VMEM((ep - 1, max(8, turn * block), cols), BF16),
-            pltpu.VMEM((ep - 1, max(8, turn * block), cols), BF16),
+            pltpu.VMEM((2,) + back, BF16),
+            pltpu.VMEM(back, BF16),
+            pltpu.VMEM(back, BF16),
             pltpu.VMEM((2, tp, block, cols), F32),
             pltpu.VMEM((chunks, block, cols), F32),
             pltpu.VMEM((chunks, chips, block, cols), BF16),
@@ -891,6 +912,10 @@
             dma((chips,)),
             dma((chips,)),
             dma((tp,)),
+            dma,
+            dma,
+            dma,
+            dma,
             dma,
             dma,
             dma,

time: 81.4 us -> 78.5 us (0.964)
  Pallas kernels: 80.4 us -> 77.3 us
    pallas_call x1, Pallas kernels: 80.4 us -> 77.3 us  [on_device(): pl.pallas_call(functools.partial(layer_kernel, (ep, tp, rows, slots, slot...]
where the time goes in v6:
time: 78.5 us; the launch traced here: 78 us
  Pallas kernels  77.3 us (98%)
    pallas_call x1, Pallas kernels, on_device(): pl.pallas_call(functools.partial(layer_kernel, (ep, tp, rows, slots, slot...  77.3 us

profile of v6, /device:TPU:0, one launch (start us, length us, event | category | flops | bytes accessed | tf_op | source)
XLA Modules:
  0.0 78.0 jit_solution(5326592095969314838)
XLA Ops:
  0.0 77.3 %moe_layer.1 = bf16[64,2048]{1,0:T(8,128)(2,1)S(1)} custom-call(bf16[512,256]{1,0:T(8,128)(2,1)} %tokens_hbm.1, s32[6,512]{1,0:T(8,128)} %bitcast.10, f32[6,512]{1,0:T(8,128)} %bitcast.11, f32[1,2048]{1,0:T(1,128)} %bitcast.12, f32[1,2048]{1,0:T(1,128)} %bitcast.13, bf16[64,2048]{1,0:T(8,128)(2,1)} %sgate_hbm.1, bf16[64,2048]{1,0:T(8,128)(2,1)} %sup_hbm.1, ...), custom_call_target="tpu_custom_call" | custom-call | tf_op jit(solution)/shard_map/moe_layer/pallas_call | solution.py:844
  77.3 0.7 copy.13

commit v7 on v6

--- a/solution.py
+++ b/solution.py
@@ -382,6 +382,11 @@
 
         lax.fori_loop(0, 4, far_step, 0)
         if not shift:
+
+            @pl.when(d == 0)
+            def _():
+                spread[...] = spread_t[...].T.astype(BF16)
+
             return carry
 
         @pl.when(d == 0)
@@ -389,6 +394,7 @@
             remote(extra.at[t], extra.at[t], x_send, x_recv, g, mate).wait_recv()
             extra_onward(z)
             pick_others()
+            spread[...] = spread_t[...].T.astype(BF16)
 
         for side in range(2):
             chip, there = at_side(side)
@@ -490,7 +496,6 @@
     su = lax.dot_general(norm[...], sup_ref[...], contract, preferred_element_type=F32)
     shidden[...] = (jax.nn.silu(sg) * su).astype(BF16)
 
-    spread[...] = spread_t[...].T.astype(BF16)
     order = near + far
 
     def expert_order(j):

time: 78.5 us -> 78.4 us (level)
  no operation moved by 1% of the time
where the time goes in v7:
time: 78.4 us; the launch traced here: 77.9 us
  Pallas kernels  77.2 us (98%)
    pallas_call x1, Pallas kernels, on_device(): pl.pallas_call(functools.partial(layer_kernel, (ep, tp, rows, slots, slot...  77.2 us

profile of v7, /device:TPU:0, one launch (start us, length us, event | category | flops | bytes accessed | tf_op | source)
XLA Modules:
  0.0 77.9 jit_solution(7863096250044934988)
XLA Ops:
  0.0 77.2 %moe_layer.1 = bf16[64,2048]{1,0:T(8,128)(2,1)S(1)} custom-call(bf16[512,256]{1,0:T(8,128)(2,1)} %tokens_hbm.1, s32[6,512]{1,0:T(8,128)} %bitcast.10, f32[6,512]{1,0:T(8,128)} %bitcast.11, f32[1,2048]{1,0:T(1,128)} %bitcast.12, f32[1,2048]{1,0:T(1,128)} %bitcast.13, bf16[64,2048]{1,0:T(8,128)(2,1)} %sgate_hbm.1, bf16[64,2048]{1,0:T(8,128)(2,1)} %sup_hbm.1, ...), custom_call_target="tpu_custom_call" | custom-call | tf_op jit(solution)/shard_map/moe_layer/pallas_call | solution.py:849
  77.2 0.7 copy.13

commit v8 on v7

--- a/solution.py
+++ b/solution.py
@@ -577,7 +577,7 @@
             def _():
                 turn_step(i + 1)
 
-            @pl.when(i == ep + 1)
+            @pl.when(i == ep)
             def _():
                 line_start()
 
@@ -720,7 +720,6 @@
 
         return carry
 
-    lax.fori_loop(0, chunks, out_step, 0)
 
     rest = pl.ds(0, chips - 1)
     if paired:
@@ -805,6 +804,8 @@
 
         else:
             remote(line_out.at[some], line_in.at[some], l_send, l_recv, g, mate).wait_send()
+
+    lax.fori_loop(0, chunks, out_step, 0)
 
 
 def on_device(

time: 78.4 us -> 78.3 us (level)
  no operation moved by 1% of the time
where the time goes in v8:
time: 78.3 us; the launch traced here: 77.8 us
  Pallas kernels  77.1 us (98%)
    pallas_call x1, Pallas kernels, on_device(): pl.pallas_call(functools.partial(layer_kernel, (ep, tp, rows, slots, slot...  77.1 us

profile of v8, /device:TPU:0, one launch (start us, length us, event | category | flops | bytes accessed | tf_op | source)
XLA Modules:
  0.0 77.8 jit_solution(15907972049780550316)
XLA Ops:
  0.0 77.1 %moe_layer.1 = bf16[64,2048]{1,0:T(8,128)(2,1)S(1)} custom-call(bf16[512,256]{1,0:T(8,128)(2,1)} %tokens_hbm.1, s32[6,512]{1,0:T(8,128)} %bitcast.10, f32[6,512]{1,0:T(8,128)} %bitcast.11, f32[1,2048]{1,0:T(1,128)} %bitcast.12, f32[1,2048]{1,0:T(1,128)} %bitcast.13, bf16[64,2048]{1,0:T(8,128)(2,1)} %sgate_hbm.1, bf16[64,2048]{1,0:T(8,128)(2,1)} %sup_hbm.1, ...), custom_call_target="tpu_custom_call" | custom-call | tf_op jit(solution)/shard_map/moe_layer/pallas_call | solution.py:850
  77.1 0.7 copy.13
